TPU v7x, 32 devices: a whole 2x2x4 slice. The times are simulated.
32 devices in a mesh: ep: 32 (over z, y, x, core).
Axes of the slice: x: 2, y: 2, z: 4, core: 2. Of those that a mesh axis runs over, the one named last changes fastest.
Arguments:
- tokens: bfloat16 [1536, 2048], P('ep'), may hold values from -6 to 6
- history_length: int32 [1536], P('ep'), may hold values from 1024 to 8192
- norm_gain: float32 [2048], replicated, may hold values from 0.1 to 1.9
- w_query: bfloat16 [2048, 512], replicated, may hold values from -0.125 to 0.125
- w_key: bfloat16 [2048, 512], replicated, may hold values from -0.125 to 0.125
- w_value: bfloat16 [2048, 512], replicated, may hold values from -0.125 to 0.125
- w_gate: bfloat16 [2048, 512], replicated, may hold values from -0.125 to 0.125
- decay_rate: float32 [8], replicated, may hold values from 0.003 to 0.7
- state: float32 [1536, 8, 64, 64], P('ep'), may hold values from -4 to 4
- head_gain: float32 [512], replicated, may hold values from 0.1 to 1.9
- w_out: bfloat16 [512, 2048], replicated, may hold values from -0.25 to 0.25
- moe_gain: float32 [2048], replicated, may hold values from 0.1 to 1.9
- route_weights: float32 [1536, 2], P('ep'), may hold values from 0.3 to 3
- expert_group: int32 [1536], P('ep'), may hold values from 0 to 3, as said below
- expert_inner: int32 [1536, 2], P('ep'), may hold values from 0 to 7, as said below
- expert_gate: bfloat16 [32, 2048, 256], P('ep'), may hold values from -0.125 to 0.125
- expert_up: bfloat16 [32, 2048, 256], P('ep'), may hold values from -0.125 to 0.125
- expert_down: bfloat16 [32, 256, 2048], P('ep'), may hold values from -0.375 to 0.375
Outputs:
- output: bfloat16 [1536, 2048], P('ep')
- new_state: float32 [1536, 8, 64, 64], P('ep')
Inputs may be any that keep to these rules, and one draw needn't show every extreme that they name: `expert_group`: together with expert_inner it names 2 different experts of one group for each token. `expert_inner`: the rows of one device name one expert at most 6 times; in every draw some expert is named exactly 6 times by the rows of every device.
All inputs are finite; a program needn't handle non-finite values.
Results may differ from a plain program's by a relative error of at most 0.02.
Values may be sent and summed in bfloat16 or wider, within the bound.
A program may use at most 128 MiB of HBM per device.

v0:
```python
import jax
import jax.numpy as jnp
import numpy as np
from jax import lax
from jax.experimental import pallas as pl
from jax.experimental.pallas import tpu as pltpu
from jax.sharding import PartitionSpec as P

GROUPS = 4
TOP_K = 2


epsilon = 1e-06


BLOCK = 8


def dot(a, b):
    return jnp.dot(a, b, preferred_element_type=jnp.float32)


def rms(values, gains):
    mean = jnp.mean(values * values, axis=-1, keepdims=True)
    return values * lax.rsqrt(mean + epsilon) * gains


def retention_kernel(
    tokens,
    history_length,
    inverse,
    norm_gain,
    decay_rate,
    head_gain,
    query_hbm,
    key_hbm,
    value_hbm,
    gate_hbm,
    out_hbm,
    state_hbm,
    mixed_out,
    new_state_hbm,
    query_w,
    key_w,
    value_w,
    gate_w,
    out_w,
    state,
    query_columns,
    key_columns,
    value_heads,
    reading,
    weight_sem,
    in_sem,
    out_sem,
):
    seq_count = tokens.shape[0]
    heads, head_width = state.shape[1], state.shape[-1]
    half = head_width // 2
    blocks = seq_count // BLOCK
    weight_copies = [
        pltpu.make_async_copy(source, target, weight_sem.at[index])
        for index, (source, target) in enumerate(
            (
                (key_hbm, key_w),
                (query_hbm, query_w),
                (value_hbm, value_w),
                (gate_hbm, gate_w),
                (out_hbm, out_w),
            )
        )
    ]

    def state_in(block):
        rows = pl.ds(block * BLOCK, BLOCK)
        return pltpu.make_async_copy(state_hbm.at[rows], state.at[rows], in_sem.at[block])

    def state_out(block):
        rows = pl.ds(block * BLOCK, BLOCK)
        return pltpu.make_async_copy(state.at[rows], new_state_hbm.at[rows], out_sem.at[block])

    for copy in weight_copies[:3]:
        copy.start()
    for block in range(blocks):
        state_in(block).start()
    for copy in weight_copies[3:]:
        copy.start()
    inputs = tokens[...].astype(jnp.float32)
    normed = rms(inputs, norm_gain[...]).astype(jnp.bfloat16)
    square = (seq_count, seq_count)
    above = lax.broadcasted_iota(jnp.int32, square, 0)
    across = lax.broadcasted_iota(jnp.int32, square, 1)
    places = history_length[...].astype(jnp.float32)
    places = jnp.sum(jnp.where(above == across, places, 0.0), axis=1, keepdims=True)
    angles = places * inverse[...]
    cosine, sine = jnp.cos(angles), jnp.sin(angles)
    cosines = jnp.concatenate([cosine] * (2 * heads), axis=1)
    sines = jnp.concatenate([-sine, sine] * heads, axis=1)
    lane = lax.broadcasted_iota(jnp.int32, cosines.shape, 1)
    leading = lax.rem(lane, head_width) < half

    def rounded(weights):
        return dot(normed, weights[...]).astype(jnp.bfloat16).astype(jnp.float32)

    def rotated(values):
        partner = jnp.where(
            leading, jnp.roll(values, -half, axis=1), jnp.roll(values, half, axis=1)
        )
        return values * cosines + partner * sines

    weight_copies[0].wait()
    keys = rotated(rounded(key_w)) * head_width ** (-0.5)
    weight_copies[1].wait()
    queries = rotated(rounded(query_w))
    for block in range(blocks):
        rows = slice(block * BLOCK, (block + 1) * BLOCK)
        key_columns[block] = keys[rows].T
        query_columns[block] = queries[rows].T
    weight_copies[2].wait()
    values = rounded(value_w)
    for head in range(heads):
        value_heads[head] = values[:, head * head_width : (head + 1) * head_width]
    retain = [
        jnp.exp(jnp.full((1, head_width), -decay_rate[head], jnp.float32)) for head in range(heads)
    ]

    def update(block, carry):
        state_in(block).wait()
        for head in range(heads):
            span = slice(head * head_width, (head + 1) * head_width)
            block_values = value_heads[head, pl.ds(block * BLOCK, BLOCK), :]
            block_keys = key_columns[block, span, :]
            block_queries = query_columns[block, span, :]
            rows = []
            for index in range(BLOCK):
                sequence = block * BLOCK + index
                fresh = (
                    retain[head] * state[sequence, head]
                    + block_keys[:, index : index + 1] * block_values[index : index + 1, :]
                )
                state[sequence, head] = fresh
                rows.append(
                    jnp.sum(block_queries[:, index : index + 1] * fresh, axis=0, keepdims=True)
                )
            reading[head, pl.ds(block * BLOCK, BLOCK), :] = jnp.concatenate(rows, axis=0)
        state_out(block).start()
        return carry

    lax.fori_loop(0, blocks, update, 0)
    weight_copies[3].wait()
    gating = rounded(gate_w)
    read = jnp.concatenate(
        [
            rms(
                reading[head],
                head_gain[:, head * head_width : (head + 1) * head_width],
            )
            for head in range(heads)
        ],
        axis=1,
    )
    mixed_heads = (read * jax.nn.silu(gating)).astype(jnp.bfloat16)
    weight_copies[4].wait()
    mixed_out[...] = (inputs + dot(mixed_heads, out_w[...])).astype(jnp.bfloat16)
    for block in range(blocks):
        state_out(block).wait()


def retention_step(
    tokens,
    history_length,
    norm_gain,
    w_query,
    w_key,
    w_value,
    w_gate,
    decay_rate,
    state,
    head_gain,
    w_out,
):
    heads = decay_rate.shape[0]
    seq_count, model_width = tokens.shape
    head_width = state.shape[-1]
    half = head_width // 2
    blocks = seq_count // BLOCK
    inverse = (10000.0 ** (-np.arange(half) / half)).astype(np.float32)
    vmem = pl.BlockSpec(memory_space=pltpu.VMEM)
    smem = pl.BlockSpec(memory_space=pltpu.SMEM)
    hbm = pl.BlockSpec(memory_space=pl.ANY)
    dma = pltpu.SemaphoreType.DMA
    f32 = jnp.float32
    row_shape = jax.ShapeDtypeStruct((seq_count, model_width), jnp.bfloat16)
    return pl.pallas_call(
        retention_kernel,
        name="retention",
        out_shape=(row_shape, jax.ShapeDtypeStruct(state.shape, f32)),
        in_specs=[vmem] * 4 + [smem, vmem] + [hbm] * 6,
        out_specs=(vmem, hbm),
        scratch_shapes=[pltpu.VMEM(w_query.shape, jnp.bfloat16)] * 4
        + [
            pltpu.VMEM(w_out.shape, jnp.bfloat16),
            pltpu.VMEM(state.shape, f32),
            pltpu.VMEM((blocks, heads * head_width, BLOCK), f32),
            pltpu.VMEM((blocks, heads * head_width, BLOCK), f32),
            pltpu.VMEM((heads, seq_count, head_width), f32),
            pltpu.VMEM((heads, seq_count, head_width), f32),
            dma((5,)),
            dma((blocks,)),
            dma((blocks,)),
        ],
        compiler_params=pltpu.CompilerParams(vmem_limit_bytes=60 * 1024 * 1024),
    )(
        tokens,
        history_length.reshape(1, -1),
        inverse.reshape(1, -1),
        norm_gain.reshape(1, -1),
        decay_rate,
        head_gain.reshape(1, -1),
        w_query,
        w_key,
        w_value,
        w_gate,
        w_out,
        state,
    )


MESH = pl.DeviceIdType.MESH
STAGES = GROUPS


def exchange_kernel(
    per_group,
    moe_gain,
    mixed,
    expert_group,
    expert_inner,
    route_weights,
    gate_hbm,
    up_hbm,
    down_hbm,
    out,
    gate_w,
    up_w,
    down_w,
    meta_send,
    meta_recv,
    zsend,
    zrecv,
    dsend,
    drecv,
    osend,
    orecv,
    csend,
    crecv,
    load_sem,
    meta_sems,
    z_sems,
    d_sems,
    o_sems,
    c_sems,
):
    device = lax.axis_index("ep")
    group = device // per_group
    inner = device % per_group
    width = zsend.shape[-1]
    group_rows = zsend.shape[1]
    peer_rows = dsend.shape[2]
    slots = GROUPS * group_rows
    rows = per_group * peer_rows

    def column_peer(step):
        other = lax.rem(group + step, GROUPS)
        return other, other * per_group + inner

    def plane_peer(step):
        other = lax.rem(inner + step, per_group)
        return other, group * per_group + other

    def send_out(step):
        other, peer = column_peer(step)
        return pltpu.make_async_remote_copy(
            src_ref=zsend.at[other],
            dst_ref=zrecv.at[step],
            send_sem=z_sems.at[0, step],
            recv_sem=z_sems.at[1, step],
            device_id=(peer,),
            device_id_type=MESH,
        )

    def send_home(step):
        home = lax.rem(group + GROUPS - step, GROUPS)
        return pltpu.make_async_remote_copy(
            src_ref=csend.at[step],
            dst_ref=crecv.at[group],
            send_sem=c_sems.at[0, step],
            recv_sem=c_sems.at[1, step],
            device_id=(home * per_group + inner,),
            device_id_type=MESH,
        )

    def plane_copy(source, target, sems, stage, step):
        other, peer = plane_peer(step)
        return pltpu.make_async_remote_copy(
            src_ref=source.at[stage, other],
            dst_ref=target.at[stage, inner],
            send_sem=sems.at[0, stage, step],
            recv_sem=sems.at[1, stage, step],
            device_id=(peer,),
            device_id_type=MESH,
        )

    def meta_copy(step):
        other, peer = column_peer(step)
        return pltpu.make_async_remote_copy(
            src_ref=meta_send.at[other],
            dst_ref=meta_recv.at[step],
            send_sem=meta_sems.at[0, step],
            recv_sem=meta_sems.at[1, step],
            device_id=(peer,),
            device_id_type=MESH,
        )

    def each_column(act):
        for step in range(1, GROUPS):
            act(step)

    def each_plane(act):
        def body(step, carry):
            act(step)
            return carry

        lax.fori_loop(1, per_group, body, 0)

    loads = [
        pltpu.make_async_copy(source, target, load_sem.at[place_index])
        for place_index, (source, target) in enumerate(
            ((gate_hbm, gate_w), (up_hbm, up_w), (down_hbm, down_w))
        )
    ]
    for load in loads:
        load.start()
    barrier = pltpu.get_barrier_semaphore()

    def greet_column(step):
        pl.semaphore_signal(barrier, inc=1, device_id=(column_peer(step)[1],), device_id_type=MESH)

    def greet_plane(step):
        pl.semaphore_signal(barrier, inc=1, device_id=(plane_peer(step)[1],), device_id_type=MESH)

    each_column(greet_column)
    each_plane(greet_plane)
    seq_count = mixed.shape[0]
    normed = rms(mixed[...].astype(jnp.float32), moe_gain[...]).astype(jnp.bfloat16)
    group_row = expert_group[...].astype(jnp.float32)
    inner_rows = [expert_inner[choice : choice + 1, :].astype(jnp.float32) for choice in (0, 1)]
    square = (seq_count, seq_count)
    above = lax.broadcasted_iota(jnp.int32, square, 0)
    across = lax.broadcasted_iota(jnp.int32, square, 1)

    def column(row):
        return jnp.sum(jnp.where(above == across, row, 0.0), axis=1, keepdims=True)

    def earlier(columns, row):
        matched = sum((values == row).astype(jnp.float32) for values in columns)
        return jnp.sum(jnp.where(above < across, matched, 0.0), axis=0, keepdims=True)

    group_slot = group_row * group_rows + earlier([column(group_row)], group_row)
    expert_rows = [group_row * per_group + row for row in inner_rows]
    expert_columns = [column(row) for row in expert_rows]
    lanes = []
    for choice in (0, 1):
        slot = earlier(expert_columns, expert_rows[choice])
        lanes.append(column(inner_rows[choice] * peer_rows + slot + 1.0))
    for choice in (0, 1):
        weight = column(route_weights[choice : choice + 1, :])
        high = weight.astype(jnp.bfloat16).astype(jnp.float32)
        lanes += [high, weight - high]
    lane = lax.broadcasted_iota(jnp.int32, (seq_count, meta_send.shape[-1]), 1)
    token_meta = jnp.zeros(lane.shape, jnp.float32)
    for index, value in enumerate(lanes):
        token_meta = jnp.where(lane == index, value, token_meta)
    slot_above = lax.broadcasted_iota(jnp.int32, (slots, seq_count), 0).astype(jnp.float32)
    slot_across = lax.broadcasted_iota(jnp.int32, (seq_count, slots), 1).astype(jnp.float32)
    placing = (slot_above == group_slot).astype(jnp.float32).astype(jnp.bfloat16)
    collecting = (slot_across == column(group_slot)).astype(jnp.float32).astype(jnp.bfloat16)
    meta = dot(placing, token_meta.astype(jnp.bfloat16)).astype(jnp.bfloat16)
    meta_send[...] = meta.reshape(meta_send.shape)
    zsend[...] = dot(placing, normed).astype(jnp.bfloat16).reshape(zsend.shape)
    pl.semaphore_wait(barrier, GROUPS - 1 + per_group - 1)
    each_column(lambda step: meta_copy(step).start())
    each_column(lambda step: send_out(step).start())
    meta_recv[0] = meta_send[group]
    zrecv[0] = zsend[group]
    weights_of = {}

    def spread_rows(stage):
        if stage:
            meta_copy(stage).wait_recv()
        meta = meta_recv[stage].astype(jnp.float32)
        row_ids = lax.broadcasted_iota(jnp.int32, (group_rows, rows), 1).astype(jnp.float32) + 1.0
        first = (row_ids == meta[:, 0:1]).astype(jnp.float32)
        second = (row_ids == meta[:, 1:2]).astype(jnp.float32)
        weights = first * (meta[:, 2:3] + meta[:, 3:4]) + second * (meta[:, 4:5] + meta[:, 5:6])
        high = weights.astype(jnp.bfloat16)
        weights_of[stage] = (high, (weights - high.astype(jnp.float32)).astype(jnp.bfloat16))
        if stage:
            send_out(stage).wait_recv()
        block = lax.dot_general(
            (first + second).astype(jnp.bfloat16),
            zrecv[stage],
            (((0,), (0,)), ((), ())),
            preferred_element_type=jnp.float32,
        ).astype(jnp.bfloat16)
        dsend[stage] = block.reshape(dsend.shape[1:])
        each_plane(lambda step: plane_copy(dsend, drecv, d_sems, stage, step).start())
        drecv[stage, inner] = dsend[stage, inner]

    def run_expert(stage):
        each_plane(lambda step: plane_copy(dsend, drecv, d_sems, stage, step).wait_recv())
        if stage == 0:
            for load in loads:
                load.wait()
        block = drecv[stage].reshape(rows, width)
        hidden = jax.nn.silu(dot(block, gate_w[...])) * dot(block, up_w[...])
        block = dot(hidden.astype(jnp.bfloat16), down_w[...]).astype(jnp.bfloat16)
        osend[stage] = block.reshape(osend.shape[1:])
        each_plane(lambda step: plane_copy(osend, orecv, o_sems, stage, step).start())
        orecv[stage, inner] = osend[stage, inner]

    def combine(stage):
        each_plane(lambda step: plane_copy(osend, orecv, o_sems, stage, step).wait_recv())
        block = orecv[stage].reshape(rows, width)
        high, low = weights_of[stage]
        csend[stage] = (dot(high, block) + dot(low, block)).astype(jnp.bfloat16)
        if stage:
            send_home(stage).start()
        else:
            crecv[group] = csend[0]

    spread_rows(0)
    spread_rows(1)
    run_expert(0)
    spread_rows(2)
    run_expert(1)
    spread_rows(3)
    combine(0)
    run_expert(2)
    combine(1)
    run_expert(3)
    combine(2)
    combine(3)
    each_column(lambda step: send_home(step).wait_recv())
    block = dot(collecting, crecv[...].reshape(slots, width))
    out[...] = (mixed[...].astype(jnp.float32) + block).astype(jnp.bfloat16)
    each_column(lambda step: meta_copy(step).wait_send())
    each_column(lambda step: send_out(step).wait_send())
    each_column(lambda step: send_home(step).wait_send())

    def drain(stage, carry):
        each_plane(lambda step: plane_copy(dsend, drecv, d_sems, stage, step).wait_send())
        each_plane(lambda step: plane_copy(osend, orecv, o_sems, stage, step).wait_send())
        return carry

    lax.fori_loop(0, STAGES, drain, 0)


def routed_experts(
    mixed_tokens, moe_gain, route_weights, expert_group, expert_inner, expert_gate, expert_up, expert_down
):
    experts = lax.axis_size("ep")
    per_group = experts // GROUPS
    seq_count, model_width = mixed_tokens.shape
    capacity = max(2, 4 * seq_count // experts)
    group_rows = -(-min(seq_count, per_group * capacity // TOP_K) // 8) * 8
    peer_rows = -(-capacity // 8) * 8
    hidden_width = expert_gate.shape[-1]
    vmem = pl.BlockSpec(memory_space=pltpu.VMEM)
    hbm = pl.BlockSpec(memory_space=pl.ANY)
    bf16 = jnp.bfloat16
    column_buffer = pltpu.VMEM((GROUPS, group_rows, model_width), bf16)
    plane_buffer = pltpu.VMEM((STAGES, per_group, peer_rows, model_width), bf16)
    meta_buffer = pltpu.VMEM((GROUPS, group_rows, 128), bf16)
    dma = pltpu.SemaphoreType.DMA

    def kernel(*refs):
        exchange_kernel(per_group, *refs)

    return pl.pallas_call(
        kernel,
        name="experts",
        out_shape=jax.ShapeDtypeStruct((seq_count, model_width), bf16),
        in_specs=[vmem] * 5 + [hbm] * 3,
        out_specs=vmem,
        scratch_shapes=[
            pltpu.VMEM((model_width, hidden_width), bf16),
            pltpu.VMEM((model_width, hidden_width), bf16),
            pltpu.VMEM((hidden_width, model_width), bf16),
            meta_buffer,
            meta_buffer,
            column_buffer,
            column_buffer,
            plane_buffer,
            plane_buffer,
            plane_buffer,
            plane_buffer,
            column_buffer,
            column_buffer,
            dma((3,)),
            dma((2, GROUPS)),
            dma((2, STAGES)),
            dma((2, STAGES, per_group)),
            dma((2, STAGES, per_group)),
            dma((2, STAGES)),
        ],
        compiler_params=pltpu.CompilerParams(
            collective_id=0,
            has_side_effects=True,
            vmem_limit_bytes=(16 + 20 * per_group // 32 * 2) * 1024 * 1024,
        ),
    )(
        moe_gain.reshape(1, -1),
        mixed_tokens,
        expert_group.reshape(1, -1),
        expert_inner.T,
        route_weights.T,
        expert_gate,
        expert_up,
        expert_down,
    )


def local(
    tokens,
    history_length,
    norm_gain,
    w_query,
    w_key,
    w_value,
    w_gate,
    decay_rate,
    state,
    head_gain,
    w_out,
    moe_gain,
    route_weights,
    expert_group,
    expert_inner,
    expert_gate,
    expert_up,
    expert_down,
):
    mixed_tokens, new_state = retention_step(
        tokens,
        history_length,
        norm_gain,
        w_query,
        w_key,
        w_value,
        w_gate,
        decay_rate,
        state,
        head_gain,
        w_out,
    )
    output = routed_experts(
        mixed_tokens,
        moe_gain,
        route_weights,
        expert_group,
        expert_inner,
        expert_gate[0],
        expert_up[0],
        expert_down[0],
    )
    return (output, new_state)


def solution(mesh):
    return jax.shard_map(
        local,
        mesh=mesh,
        in_specs=(
            P("ep", None),
            P("ep"),
            P(),
            P(),
            P(),
            P(),
            P(),
            P(),
            P("ep", None, None, None),
            P(),
            P(),
            P(),
            P("ep", None),
            P("ep"),
            P("ep", None),
            P("ep", None, None),
            P("ep", None, None),
            P("ep", None, None),
        ),
        out_specs=(P("ep", None), P("ep", None, None, None)),
        check_vma=False,
    )
```

profile of v0, /device:TPU:0, one launch (start us, length us, event | category | flops | bytes accessed | tf_op | source)
XLA Modules:
  0.0 58.8 jit_solution(18323207379902139247)
XLA Ops:
  0.6 0.0 copy-start
  0.6 0.0 copy-start.1
  0.7 0.0 copy-start.2
  0.7 0.0 copy-start.4
  0.7 0.0 copy-start.5
  0.7 0.0 copy-start.6
  0.7 0.0 copy-start.7
  0.7 16.1 %retention.1 = (bf16[48,2048]{1,0:T(8,128)(2,1)}, f32[48,8,64,64]{3,2,1,0:T(8,128)}) custom-call(bf16[48,2048]{1,0:T(8,128)(2,1)} %tokens.1, s32[1,48]{1,0:T(1,128)} %bitcast.19, f32[1,32]{1,0:T(1,128)} %constant.2.clone.inverse, f32[1,2048]{1,0:T(1,128)} %bitcast.17, f32[8]{0:T(128)} %decay_rate.1, f32[1,512]{1,0:T(1,128)} %bitcast.18, ...), custom_call_target="tpu_custom_call" | custom-call | tf_op jit(solution)/shard_map/retention/pallas_call | solution.py:194
  16.8 0.0 copy-done
  16.8 0.0 copy-done.1
  16.8 0.0 copy-done.2
  16.8 0.0 copy-done.4
  16.8 0.0 copy-done.5
  16.8 0.0 copy-done.6
  16.9 0.0 copy-done.7
  16.9 0.0 copy-start.3
  16.9 0.9 %copy-done.3 = bf16[48,2048]{1,0:T(8,128)(2,1)S(1)} copy-done((bf16[48,2048]{1,0:T(8,128)(2,1)S(1)}, bf16[48,2048]{1,0:T(8,128)(2,1)}, u32[]{:S(2)}) %copy-start.3) | copy-done | bytes 196632
  17.8 40.3 %experts.1 = bf16[48,2048]{1,0:T(8,128)(2,1)S(1)} custom-call(f32[1,2048]{1,0:T(1,128)S(1)} %bitcast.13, bf16[48,2048]{1,0:T(8,128)(2,1)S(1)} %copy-done.3, s32[1,48]{1,0:T(1,128)S(1)} %bitcast.16, s32[2,48]{1,0:T(2,128)S(1)} %bitcast.14, f32[2,48]{1,0:T(2,128)S(1)} %bitcast.15, bf16[2048,256]{1,0:T(8,128)(2,1)S(1)} %bitcast.10, ...), custom_call_target="tpu_custom_call" | custom-call | tf_op jit(solution)/shard_map/experts/pallas_call | solution.py:490
  58.1 0.7 %copy.22 = bf16[48,2048]{1,0:T(8,128)(2,1)} copy(bf16[48,2048]{1,0:T(8,128)(2,1)S(1)} %experts.1) | data formatting | bytes 393216
Async XLA Ops:
  0.6 16.2 %copy-start = (bf16[1,2048,256]{2,1,0:T(8,128)(2,1)S(1)}, bf16[1,2048,256]{2,1,0:T(8,128)(2,1)}, u32[]{:S(2)}) copy-start(bf16[1,2048,256]{2,1,0:T(8,128)(2,1)} %param.34) | copy-start | bytes 3145732
  0.6 16.2 %copy-start.1 = (bf16[1,2048,256]{2,1,0:T(8,128)(2,1)S(1)}, bf16[1,2048,256]{2,1,0:T(8,128)(2,1)}, u32[]{:S(2)}) copy-start(bf16[1,2048,256]{2,1,0:T(8,128)(2,1)} %param.35) | copy-start | bytes 3145732
  0.7 16.2 %copy-start.2 = (bf16[1,256,2048]{2,1,0:T(8,128)(2,1)S(1)}, bf16[1,256,2048]{2,1,0:T(8,128)(2,1)}, u32[]{:S(2)}) copy-start(bf16[1,256,2048]{2,1,0:T(8,128)(2,1)} %param.36) | copy-start | bytes 3145732
  0.7 16.2 %copy-start.4 = (f32[2048]{0:T(1024)S(1)}, f32[2048]{0:T(1024)}, u32[]{:S(2)}) copy-start(f32[2048]{0:T(1024)} %param.30) | copy-start | bytes 24580
  0.7 16.2 %copy-start.5 = (s32[48,2]{0,1:T(2,128)S(1)}, s32[48,2]{0,1:T(2,128)}, u32[]{:S(2)}) copy-start(s32[48,2]{0,1:T(2,128)} %param.33) | copy-start | bytes 1156
  0.7 16.2 %copy-start.6 = (f32[48,2]{0,1:T(2,128)S(1)}, f32[48,2]{0,1:T(2,128)}, u32[]{:S(2)}) copy-start(f32[48,2]{0,1:T(2,128)} %param.31) | copy-start | bytes 1156
  0.7 16.2 %copy-start.7 = (s32[48]{0:T(128)S(1)}, s32[48]{0:T(128)}, u32[]{:S(2)}) copy-start(s32[48]{0:T(128)} %param.32) | copy-start | bytes 580
  16.9 0.9 %copy-start.3 = (bf16[48,2048]{1,0:T(8,128)(2,1)S(1)}, bf16[48,2048]{1,0:T(8,128)(2,1)}, u32[]{:S(2)}) copy-start(bf16[48,2048]{1,0:T(8,128)(2,1)} %get-tuple-element.4.refs_1_) | copy-start | bytes 589828
where the time goes:
time: 58.9 us; the launch traced here: 58.8 us
  Pallas kernels  56.4 us (96%)
  local copies, waits for them, and re-layouts  1.63 us (3%)
  between operations  0.77 us (1%)
    pallas_call x1, Pallas kernels, routed_experts(): pl.pallas_call(kernel, name='experts', out_shape=jax.ShapeDtypeStruct((se...  40.3 us
    pallas_call x1, Pallas kernels, retention_step(): pl.pallas_call(retention_kernel, name='retention', out_shape=(row_shape,...  16.1 us
    unnamed x17, local copies, waits for them, and re-layouts  1.63 us

commit v1 on v0

v1 whole, which is shorter than its diff:
```python
import jax
import jax.numpy as jnp
import numpy as np
from jax import lax
from jax.experimental import pallas as pl
from jax.experimental.pallas import tpu as pltpu
from jax.sharding import PartitionSpec as P

GROUPS = 4
TOP_K = 2


epsilon = 1e-06


BLOCK = 8


MESH = pl.DeviceIdType.MESH
STAGES = GROUPS


def dot(a, b):
    return jnp.dot(a, b, preferred_element_type=jnp.float32)


def rms(values, gains):
    mean = jnp.mean(values * values, axis=-1, keepdims=True)
    return values * lax.rsqrt(mean + epsilon) * gains


def layer_kernel(
    per_group,
    tokens,
    history_length,
    inverse,
    norm_gain,
    decay_rate,
    head_gain,
    moe_gain,
    expert_group,
    expert_inner,
    route_weights,
    query_hbm,
    key_hbm,
    value_hbm,
    gate_hbm,
    out_hbm,
    state_hbm,
    expert_gate_hbm,
    expert_up_hbm,
    expert_down_hbm,
    out,
    state,
    query_w,
    key_w,
    value_w,
    gate_w,
    out_w,
    expert_gate_w,
    expert_up_w,
    expert_down_w,
    query_columns,
    key_columns,
    value_heads,
    reading,
    meta_send,
    meta_recv,
    zsend,
    zrecv,
    hsend,
    hrecv,
    dsend,
    drecv,
    esend,
    erecv,
    osend,
    orecv,
    csend,
    crecv,
    weight_sem,
    in_sem,
    load_sem,
    meta_sems,
    z_sems,
    h_sems,
    d_sems,
    e_sems,
    o_sems,
    c_sems,
):
    device = lax.axis_index("ep")
    group = device // per_group
    inner = device % per_group
    seq_count, width = tokens.shape
    group_rows = zsend.shape[1]
    peer_rows = dsend.shape[2]
    slots = GROUPS * group_rows
    rows = per_group * peer_rows
    heads, head_width = state.shape[1], state.shape[-1]
    half = head_width // 2
    blocks = seq_count // BLOCK

    def column_peer(step):
        other = lax.rem(group + step, GROUPS)
        return other, other * per_group + inner

    def plane_peer(step):
        other = lax.rem(inner + step, per_group)
        return other, group * per_group + other

    def remote(source, target, send_sem, recv_sem, peer):
        return pltpu.make_async_remote_copy(
            src_ref=source,
            dst_ref=target,
            send_sem=send_sem,
            recv_sem=recv_sem,
            device_id=(peer,),
            device_id_type=MESH,
        )

    def column_copy(source, target, sems, step):
        other, peer = column_peer(step)
        return remote(source.at[other], target.at[step], sems.at[0, step], sems.at[1, step], peer)

    def send_home(step):
        home = lax.rem(group + GROUPS - step, GROUPS)
        return remote(
            csend.at[step],
            crecv.at[group],
            c_sems.at[0, step],
            c_sems.at[1, step],
            home * per_group + inner,
        )

    def plane_copy(source, target, sems, stage, step):
        other, peer = plane_peer(step)
        return remote(
            source.at[stage, other],
            target.at[stage, inner],
            sems.at[0, stage, step],
            sems.at[1, stage, step],
            peer,
        )

    def each_column(act):
        for step in range(1, GROUPS):
            act(step)

    def each_plane(act):
        def body(step, carry):
            act(step)
            return carry

        lax.fori_loop(1, per_group, body, 0)

    def load_all(pairs, sem):
        return [
            pltpu.make_async_copy(source, target, sem.at[index])
            for index, (source, target) in enumerate(pairs)
        ]

    weight_copies = load_all(
        (
            (key_hbm, key_w),
            (query_hbm, query_w),
            (value_hbm, value_w),
            (gate_hbm, gate_w),
            (out_hbm, out_w),
        ),
        weight_sem,
    )
    loads = load_all(
        (
            (expert_gate_hbm, expert_gate_w),
            (expert_up_hbm, expert_up_w),
            (expert_down_hbm, expert_down_w),
        ),
        load_sem,
    )

    def state_in(block):
        span = pl.ds(block * BLOCK, BLOCK)
        return pltpu.make_async_copy(state_hbm.at[span], state.at[span], in_sem.at[block])

    for copy in weight_copies[:3]:
        copy.start()
    for block in range(blocks):
        state_in(block).start()
    for copy in weight_copies[3:]:
        copy.start()
    for load in loads:
        load.start()

    barrier = pltpu.get_barrier_semaphore()

    def greet_column(step):
        pl.semaphore_signal(barrier, inc=1, device_id=(column_peer(step)[1],), device_id_type=MESH)

    def greet_plane(step):
        pl.semaphore_signal(barrier, inc=1, device_id=(plane_peer(step)[1],), device_id_type=MESH)

    each_column(greet_column)
    each_plane(greet_plane)

    square = (seq_count, seq_count)
    above = lax.broadcasted_iota(jnp.int32, square, 0)
    across = lax.broadcasted_iota(jnp.int32, square, 1)

    def column(row):
        return jnp.sum(jnp.where(above == across, row, 0.0), axis=1, keepdims=True)

    def earlier(columns, row):
        matched = sum((values == row).astype(jnp.float32) for values in columns)
        return jnp.sum(jnp.where(above < across, matched, 0.0), axis=0, keepdims=True)

    group_row = expert_group[...].astype(jnp.float32)
    inner_rows = [expert_inner[choice : choice + 1, :].astype(jnp.float32) for choice in (0, 1)]
    group_slot = group_row * group_rows + earlier([column(group_row)], group_row)
    expert_rows = [group_row * per_group + row for row in inner_rows]
    expert_columns = [column(row) for row in expert_rows]
    lanes = []
    for choice in (0, 1):
        slot = earlier(expert_columns, expert_rows[choice])
        lanes.append(column(inner_rows[choice] * peer_rows + slot + 1.0))
    for choice in (0, 1):
        weight = column(route_weights[choice : choice + 1, :])
        high = weight.astype(jnp.bfloat16).astype(jnp.float32)
        lanes += [high, weight - high]
    lane = lax.broadcasted_iota(jnp.int32, (seq_count, meta_send.shape[-1]), 1)
    token_meta = jnp.zeros(lane.shape, jnp.float32)
    for index, value in enumerate(lanes):
        token_meta = jnp.where(lane == index, value, token_meta)
    slot_above = lax.broadcasted_iota(jnp.int32, (slots, seq_count), 0).astype(jnp.float32)
    slot_across = lax.broadcasted_iota(jnp.int32, (seq_count, slots), 1).astype(jnp.float32)
    placing = (slot_above == group_slot).astype(jnp.float32).astype(jnp.bfloat16)
    collecting = (slot_across == column(group_slot)).astype(jnp.float32).astype(jnp.bfloat16)
    meta = dot(placing, token_meta.astype(jnp.bfloat16)).astype(jnp.bfloat16)
    meta_send[...] = meta.reshape(meta_send.shape)
    zsend[...] = dot(placing, tokens[...]).astype(jnp.bfloat16).reshape(zsend.shape)
    pl.semaphore_wait(barrier, GROUPS - 1 + per_group - 1)
    each_column(lambda step: column_copy(meta_send, meta_recv, meta_sems, step).start())
    each_column(lambda step: column_copy(zsend, zrecv, z_sems, step).start())
    meta_recv[0] = meta_send[group]
    zrecv[0] = zsend[group]
    picks_of = {}
    weights_of = {}

    def route(stage):
        if stage:
            column_copy(meta_send, meta_recv, meta_sems, stage).wait_recv()
        meta = meta_recv[stage].astype(jnp.float32)
        row_ids = lax.broadcasted_iota(jnp.int32, (group_rows, rows), 1).astype(jnp.float32) + 1.0
        first = (row_ids == meta[:, 0:1]).astype(jnp.float32)
        second = (row_ids == meta[:, 1:2]).astype(jnp.float32)
        weights = first * (meta[:, 2:3] + meta[:, 3:4]) + second * (meta[:, 4:5] + meta[:, 5:6])
        high = weights.astype(jnp.bfloat16)
        picks_of[stage] = (first + second).astype(jnp.bfloat16)
        weights_of[stage] = (high, (weights - high.astype(jnp.float32)).astype(jnp.bfloat16))

    def spread(stage, received, sent, landed, sems):
        block = lax.dot_general(
            picks_of[stage],
            received[stage],
            (((0,), (0,)), ((), ())),
            preferred_element_type=jnp.float32,
        ).astype(jnp.bfloat16)
        sent[stage] = block.reshape(sent.shape[1:])
        each_plane(lambda step: plane_copy(sent, landed, sems, stage, step).start())
        landed[stage, inner] = sent[stage, inner]

    def spread_tokens(stage):
        route(stage)
        if stage:
            column_copy(zsend, zrecv, z_sems, stage).wait_recv()
        spread(stage, zrecv, dsend, drecv, d_sems)

    def spread_heads(stage):
        if stage:
            column_copy(hsend, hrecv, h_sems, stage).wait_recv()
        spread(stage, hrecv, esend, erecv, e_sems)

    spread_tokens(0)

    inputs = tokens[...].astype(jnp.float32)
    normed = rms(inputs, norm_gain[...]).astype(jnp.bfloat16)
    places = column(history_length[...].astype(jnp.float32))
    angles = places * inverse[...]
    cosine, sine = jnp.cos(angles), jnp.sin(angles)
    cosines = jnp.concatenate([cosine] * (2 * heads), axis=1)
    sines = jnp.concatenate([-sine, sine] * heads, axis=1)
    head_lane = lax.broadcasted_iota(jnp.int32, cosines.shape, 1)
    leading = lax.rem(head_lane, head_width) < half

    def rounded(weights):
        return dot(normed, weights[...]).astype(jnp.bfloat16).astype(jnp.float32)

    def rotated(values):
        partner = jnp.where(
            leading, jnp.roll(values, -half, axis=1), jnp.roll(values, half, axis=1)
        )
        return values * cosines + partner * sines

    weight_copies[0].wait()
    keys = rotated(rounded(key_w)) * head_width ** (-0.5)
    weight_copies[1].wait()
    queries = rotated(rounded(query_w))
    for block in range(blocks):
        span = slice(block * BLOCK, (block + 1) * BLOCK)
        key_columns[block] = keys[span].T
        query_columns[block] = queries[span].T
    weight_copies[2].wait()
    values = rounded(value_w)
    for head in range(heads):
        value_heads[head] = values[:, head * head_width : (head + 1) * head_width]
    retain = [
        jnp.exp(jnp.full((1, head_width), -decay_rate[head], jnp.float32)) for head in range(heads)
    ]

    def update(block, carry):
        state_in(block).wait()
        for head in range(heads):
            span = slice(head * head_width, (head + 1) * head_width)
            block_values = value_heads[head, pl.ds(block * BLOCK, BLOCK), :]
            block_keys = key_columns[block, span, :]
            block_queries = query_columns[block, span, :]
            read_rows = []
            for index in range(BLOCK):
                sequence = block * BLOCK + index
                fresh = (
                    retain[head] * state[sequence, head]
                    + block_keys[:, index : index + 1] * block_values[index : index + 1, :]
                )
                state[sequence, head] = fresh
                read_rows.append(
                    jnp.sum(block_queries[:, index : index + 1] * fresh, axis=0, keepdims=True)
                )
            reading[head, pl.ds(block * BLOCK, BLOCK), :] = jnp.concatenate(read_rows, axis=0)
        return carry

    lax.fori_loop(0, blocks // 2, update, 0)
    spread_tokens(1)
    lax.fori_loop(blocks // 2, blocks, update, 0)
    weight_copies[3].wait()
    gating = rounded(gate_w)
    read = jnp.concatenate(
        [
            rms(
                reading[head],
                head_gain[:, head * head_width : (head + 1) * head_width],
            )
            for head in range(heads)
        ],
        axis=1,
    )
    mixed_heads = (read * jax.nn.silu(gating)).astype(jnp.bfloat16)
    hsend[...] = dot(placing, mixed_heads).astype(jnp.bfloat16).reshape(hsend.shape)
    each_column(lambda step: column_copy(hsend, hrecv, h_sems, step).start())
    hrecv[0] = hsend[group]
    spread_heads(0)
    spread_tokens(2)
    spread_tokens(3)
    weight_copies[4].wait()
    mixed = (inputs + dot(mixed_heads, out_w[...])).astype(jnp.bfloat16)
    for stage in range(1, STAGES):
        spread_heads(stage)
    for load in loads:
        load.wait()

    def run_expert(stage):
        each_plane(lambda step: plane_copy(dsend, drecv, d_sems, stage, step).wait_recv())
        each_plane(lambda step: plane_copy(esend, erecv, e_sems, stage, step).wait_recv())
        token_rows = drecv[stage].reshape(rows, width).astype(jnp.float32)
        head_rows = erecv[stage].reshape(rows, erecv.shape[-1])
        block = (token_rows + dot(head_rows, out_w[...])).astype(jnp.bfloat16)
        block = rms(block.astype(jnp.float32), moe_gain[...]).astype(jnp.bfloat16)
        hidden = jax.nn.silu(dot(block, expert_gate_w[...])) * dot(block, expert_up_w[...])
        block = dot(hidden.astype(jnp.bfloat16), expert_down_w[...]).astype(jnp.bfloat16)
        osend[stage] = block.reshape(osend.shape[1:])

    def send_back(stage):
        each_plane(lambda step: plane_copy(osend, orecv, o_sems, stage, step).start())
        orecv[stage, inner] = osend[stage, inner]

    def combine(stage):
        each_plane(lambda step: plane_copy(osend, orecv, o_sems, stage, step).wait_recv())
        block = orecv[stage].reshape(rows, width)
        high, low = weights_of[stage]
        csend[stage] = (dot(high, block) + dot(low, block)).astype(jnp.bfloat16)
        if stage:
            send_home(stage).start()
        else:
            crecv[group] = csend[0]

    run_expert(0)
    run_expert(1)
    send_back(1)
    run_expert(2)
    send_back(2)
    run_expert(3)
    send_back(3)
    send_back(0)
    combine(1)
    combine(2)
    combine(3)
    combine(0)
    each_column(lambda step: send_home(step).wait_recv())
    block = dot(collecting, crecv[...].reshape(slots, width))
    out[...] = (mixed.astype(jnp.float32) + block).astype(jnp.bfloat16)
    each_column(lambda step: column_copy(meta_send, meta_recv, meta_sems, step).wait_send())
    each_column(lambda step: column_copy(zsend, zrecv, z_sems, step).wait_send())
    each_column(lambda step: column_copy(hsend, hrecv, h_sems, step).wait_send())
    each_column(lambda step: send_home(step).wait_send())

    def drain(stage, carry):
        each_plane(lambda step: plane_copy(dsend, drecv, d_sems, stage, step).wait_send())
        each_plane(lambda step: plane_copy(esend, erecv, e_sems, stage, step).wait_send())
        each_plane(lambda step: plane_copy(osend, orecv, o_sems, stage, step).wait_send())
        return carry

    lax.fori_loop(0, STAGES, drain, 0)


def local(
    tokens,
    history_length,
    norm_gain,
    w_query,
    w_key,
    w_value,
    w_gate,
    decay_rate,
    state,
    head_gain,
    w_out,
    moe_gain,
    route_weights,
    expert_group,
    expert_inner,
    expert_gate,
    expert_up,
    expert_down,
):
    experts = lax.axis_size("ep")
    per_group = experts // GROUPS
    heads = decay_rate.shape[0]
    seq_count, model_width = tokens.shape
    head_width = state.shape[-1]
    mixed_width = heads * head_width
    half = head_width // 2
    blocks = seq_count // BLOCK
    inverse = (10000.0 ** (-np.arange(half) / half)).astype(np.float32)
    capacity = max(2, 4 * seq_count // experts)
    group_rows = -(-min(seq_count, per_group * capacity // TOP_K) // 8) * 8
    peer_rows = -(-capacity // 8) * 8
    vmem = pl.BlockSpec(memory_space=pltpu.VMEM)
    smem = pl.BlockSpec(memory_space=pltpu.SMEM)
    hbm = pl.BlockSpec(memory_space=pl.ANY)
    dma = pltpu.SemaphoreType.DMA
    bf16, f32 = jnp.bfloat16, jnp.float32

    def column_buffer(lanes):
        return [pltpu.VMEM((GROUPS, group_rows, lanes), bf16)] * 2

    def plane_buffer(lanes):
        return [pltpu.VMEM((STAGES, per_group, peer_rows, lanes), bf16)] * 2

    weights = (w_query, w_key, w_value, w_gate, w_out, expert_gate[0], expert_up[0], expert_down[0])
    state_bytes = state.size // head_width * max(head_width, 128) * 4

    def kernel(*refs):
        layer_kernel(per_group, *refs)

    output, new_state = pl.pallas_call(
        kernel,
        name="layer",
        out_shape=(
            jax.ShapeDtypeStruct((seq_count, model_width), bf16),
            pltpu.VMEM(state.shape, f32),
        ),
        in_specs=[vmem] * 4 + [smem] + [vmem] * 5 + [hbm] * 9,
        out_specs=(vmem, vmem),
        scratch_shapes=[pltpu.VMEM(weight.shape, bf16) for weight in weights]
        + [
            pltpu.VMEM((blocks, mixed_width, BLOCK), f32),
            pltpu.VMEM((blocks, mixed_width, BLOCK), f32),
            pltpu.VMEM((heads, seq_count, head_width), f32),
            pltpu.VMEM((heads, seq_count, head_width), f32),
        ]
        + column_buffer(128)
        + column_buffer(model_width)
        + column_buffer(mixed_width)
        + plane_buffer(model_width)
        + plane_buffer(mixed_width)
        + plane_buffer(model_width)
        + column_buffer(model_width)
        + [
            dma((5,)),
            dma((blocks,)),
            dma((3,)),
            dma((2, GROUPS)),
            dma((2, GROUPS)),
            dma((2, GROUPS)),
            dma((2, STAGES, per_group)),
            dma((2, STAGES, per_group)),
            dma((2, STAGES, per_group)),
            dma((2, STAGES)),
        ],
        compiler_params=pltpu.CompilerParams(
            collective_id=0,
            has_side_effects=True,
            vmem_limit_bytes=63 * 1024 * 1024 - state_bytes,
        ),
    )(
        tokens,
        history_length.reshape(1, -1),
        inverse.reshape(1, -1),
        norm_gain.reshape(1, -1),
        decay_rate,
        head_gain.reshape(1, -1),
        moe_gain.reshape(1, -1),
        expert_group.reshape(1, -1),
        expert_inner.T,
        route_weights.T,
        w_query,
        w_key,
        w_value,
        w_gate,
        w_out,
        state,
        expert_gate[0],
        expert_up[0],
        expert_down[0],
    )
    return (output, new_state)


def solution(mesh):
    return jax.shard_map(
        local,
        mesh=mesh,
        in_specs=(
            P("ep", None),
            P("ep"),
            P(),
            P(),
            P(),
            P(),
            P(),
            P(),
            P("ep", None, None, None),
            P(),
            P(),
            P(),
            P("ep", None),
            P("ep"),
            P("ep", None),
            P("ep", None, None),
            P("ep", None, None),
            P("ep", None, None),
        ),
        out_specs=(P("ep", None), P("ep", None, None, None)),
        check_vma=False,
    )
```

time: 58.9 us -> 55.7 us (0.946)
  Pallas kernels: 56.4 us -> 49.1 us
  local copies, waits for them, and re-layouts: 1.63 us -> 5.46 us
    pallas_call x2 -> x1, Pallas kernels: 56.4 us -> 49.1 us  [local(): pl.pallas_call(kernel, name='layer', out_shape=(jax.ShapeDtypeStruct((seq...]
    unnamed x17 -> x4, local copies, waits for them, and re-layouts: 1.63 us -> 5.46 us
where the time goes in v1:
time: 55.7 us; the launch traced here: 55.2 us
  Pallas kernels  49.1 us (88%)
  local copies, waits for them, and re-layouts  5.46 us (10%)
  between operations  0.65 us (1%)
    pallas_call x1, Pallas kernels, local(): pl.pallas_call(kernel, name='layer', out_shape=(jax.ShapeDtypeStruct((seq...  49.1 us
    unnamed x4, local copies, waits for them, and re-layouts  5.46 us

profile of v1, /device:TPU:0, one launch (start us, length us, event | category | flops | bytes accessed | tf_op | source)
XLA Modules:
  0.0 55.2 jit_solution(15316665124533760987)
XLA Ops:
  0.6 49.1 %layer.1 = (bf16[48,2048]{1,0:T(8,128)(2,1)}, f32[48,8,64,64]{3,2,1,0:T(8,128)S(1)}) custom-call(bf16[48,2048]{1,0:T(8,128)(2,1)} %refs_0_.1, s32[1,48]{1,0:T(1,128)} %bitcast.18, f32[1,32]{1,0:T(1,128)} %constant.2.clone.refs_2_, f32[1,2048]{1,0:T(1,128)} %bitcast.13, f32[8]{0:T(128)} %refs_4_.1, f32[1,512]{1,0:T(1,128)} %bitcast.15, f32[1,2048]{1,0:T(1,128)} %bitcast.14, ...), custom_call_target="tpu_custom_call" | custom-call | tf_op jit(solution)/shard_map/layer/pallas_call | solution.py:474
  49.7 0.0 copy-start
  49.7 4.8 %copy.23 = f32[48,8,64,64]{3,2,1,0:T(8,128)} copy(f32[48,8,64,64]{3,2,1,0:T(8,128)S(1)} %get-tuple-element.3) | data formatting | bytes 12582912
  54.5 0.0 copy-done
  54.5 0.7 %copy.24 = bf16[48,2048]{1,0:T(8,128)(2,1)} copy(bf16[48,2048]{1,0:T(8,128)(2,1)S(1)} %copy-done) | data formatting | bytes 393216
Async XLA Ops:
  49.7 4.8 %copy-start = (bf16[48,2048]{1,0:T(8,128)(2,1)S(1)}, bf16[48,2048]{1,0:T(8,128)(2,1)}, u32[]{:S(2)}) copy-start(bf16[48,2048]{1,0:T(8,128)(2,1)} %get-tuple-element.6) | copy-start | bytes 589828

commit v2 on v1

--- a/solution.py
+++ b/solution.py
@@ -18,6 +18,8 @@
 
 MESH = pl.DeviceIdType.MESH
 STAGES = GROUPS
+QUARTERS = 4
+ORDER = (2, 1, 3)
 
 
 def dot(a, b):
@@ -31,6 +33,7 @@
 
 def layer_kernel(
     per_group,
+    capacity,
     tokens,
     history_length,
     inverse,
@@ -64,6 +67,7 @@
     key_columns,
     value_heads,
     reading,
+    overlap,
     meta_send,
     meta_recv,
     zsend,
@@ -94,9 +98,10 @@
     inner = device % per_group
     seq_count, width = tokens.shape
     group_rows = zsend.shape[1]
-    peer_rows = dsend.shape[2]
     slots = GROUPS * group_rows
-    rows = per_group * peer_rows
+    rows = per_group * capacity
+    tiles = per_group * BLOCK
+    parts = capacity * QUARTERS // BLOCK
     heads, head_width = state.shape[1], state.shape[-1]
     half = head_width // 2
     blocks = seq_count // BLOCK
@@ -138,13 +143,23 @@
         return remote(
             source.at[stage, other],
             target.at[stage, inner],
-            sems.at[0, stage, step],
-            sems.at[1, stage, step],
+            sems.at[0, stage],
+            sems.at[1, stage],
             peer,
         )
 
+    def plane_total(source, target, sems, stage):
+        others = pl.ds(0, per_group - 1)
+        return remote(
+            source.at[stage, others],
+            target.at[stage, others],
+            sems.at[0, stage],
+            sems.at[1, stage],
+            plane_peer(1)[1],
+        )
+
     def each_column(act):
-        for step in range(1, GROUPS):
+        for step in ORDER:
             act(step)
 
     def each_plane(act):
@@ -222,7 +237,7 @@
     lanes = []
     for choice in (0, 1):
         slot = earlier(expert_columns, expert_rows[choice])
-        lanes.append(column(inner_rows[choice] * peer_rows + slot + 1.0))
+        lanes.append(column(inner_rows[choice] * capacity + slot + 1.0))
     for choice in (0, 1):
         weight = column(route_weights[choice : choice + 1, :])
         high = weight.astype(jnp.bfloat16).astype(jnp.float32)
@@ -238,34 +253,76 @@
     meta = dot(placing, token_meta.astype(jnp.bfloat16)).astype(jnp.bfloat16)
     meta_send[...] = meta.reshape(meta_send.shape)
     zsend[...] = dot(placing, tokens[...]).astype(jnp.bfloat16).reshape(zsend.shape)
-    pl.semaphore_wait(barrier, GROUPS - 1 + per_group - 1)
+    with jax.named_scope("barrier"):
+        pl.semaphore_wait(barrier, GROUPS - 1 + per_group - 1)
     each_column(lambda step: column_copy(meta_send, meta_recv, meta_sems, step).start())
     each_column(lambda step: column_copy(zsend, zrecv, z_sems, step).start())
     meta_recv[0] = meta_send[group]
     zrecv[0] = zsend[group]
+    def packed_places(shape, axis):
+        index = lax.broadcasted_iota(jnp.int32, shape, axis)
+        part = sum((index >= tiles * bound).astype(jnp.int32) for bound in range(1, parts))
+        index = index - part * tiles
+        place = (index & (BLOCK - 1)) * parts + part
+        return (index >> 3) * capacity + (place >> 2), place & (QUARTERS - 1)
+
+    packed_rows, packed_quarter = packed_places((1, parts * tiles), 1)
+    row_names = packed_rows.astype(jnp.float32) + 1.0
+    in_quarter = [(packed_quarter == part).astype(jnp.float32) for part in range(QUARTERS)]
+    row_number = lax.broadcasted_iota(jnp.int32, (rows, parts * tiles), 0)
+    same_row = (row_number == packed_rows).astype(jnp.float32)
+    packing = jnp.concatenate([same_row * part for part in in_quarter], axis=0).astype(jnp.bfloat16)
     picks_of = {}
     weights_of = {}
+
+    def stacked(block):
+        share = block.shape[-1] // QUARTERS
+        return jnp.concatenate(
+            [block[:, part * share : (part + 1) * share] for part in range(QUARTERS)], axis=0
+        )
+
+    def unstacked(block):
+        share = block.shape[0] // QUARTERS
+        return jnp.concatenate(
+            [block[part * share : (part + 1) * share] for part in range(QUARTERS)], axis=1
+        )
+
+    def take(picks, block):
+        return lax.dot_general(
+            picks, block, (((0,), (0,)), ((), ())), preferred_element_type=jnp.float32
+        ).astype(jnp.bfloat16)
+
+    def store_packed(sent, stage, block):
+        share = block.shape[-1]
+        for part in range(parts):
+            sent[stage, :, :, part * share : (part + 1) * share] = block[
+                part * tiles : (part + 1) * tiles
+            ].reshape(per_group, BLOCK, share)
+
+    def load_packed(landed, stage):
+        block = landed[stage].reshape(tiles, landed.shape[-1])
+        share = block.shape[-1] // parts
+        return jnp.concatenate(
+            [block[:, part * share : (part + 1) * share] for part in range(parts)], axis=0
+        )
 
     def route(stage):
         if stage:
             column_copy(meta_send, meta_recv, meta_sems, stage).wait_recv()
         meta = meta_recv[stage].astype(jnp.float32)
-        row_ids = lax.broadcasted_iota(jnp.int32, (group_rows, rows), 1).astype(jnp.float32) + 1.0
-        first = (row_ids == meta[:, 0:1]).astype(jnp.float32)
-        second = (row_ids == meta[:, 1:2]).astype(jnp.float32)
+        first = (row_names == meta[:, 0:1]).astype(jnp.float32)
+        second = (row_names == meta[:, 1:2]).astype(jnp.float32)
         weights = first * (meta[:, 2:3] + meta[:, 3:4]) + second * (meta[:, 4:5] + meta[:, 5:6])
+        both = first + second
+        picks = jnp.concatenate([both * part for part in in_quarter], axis=0)
+        weights = jnp.concatenate([weights * part for part in in_quarter], axis=0)
         high = weights.astype(jnp.bfloat16)
-        picks_of[stage] = (first + second).astype(jnp.bfloat16)
+        picks_of[stage] = picks.astype(jnp.bfloat16)
         weights_of[stage] = (high, (weights - high.astype(jnp.float32)).astype(jnp.bfloat16))
 
     def spread(stage, received, sent, landed, sems):
-        block = lax.dot_general(
-            picks_of[stage],
-            received[stage],
-            (((0,), (0,)), ((), ())),
-            preferred_element_type=jnp.float32,
-        ).astype(jnp.bfloat16)
-        sent[stage] = block.reshape(sent.shape[1:])
+        block = stacked(received[stage].astype(jnp.float32)).astype(jnp.bfloat16)
+        store_packed(sent, stage, take(picks_of[stage], block))
         each_plane(lambda step: plane_copy(sent, landed, sems, stage, step).start())
         landed[stage, inner] = sent[stage, inner]
 
@@ -280,7 +337,8 @@
             column_copy(hsend, hrecv, h_sems, stage).wait_recv()
         spread(stage, hrecv, esend, erecv, e_sems)
 
-    spread_tokens(0)
+    with jax.named_scope("spread_tokens_0"):
+        spread_tokens(0)
 
     inputs = tokens[...].astype(jnp.float32)
     normed = rms(inputs, norm_gain[...]).astype(jnp.bfloat16)
@@ -301,15 +359,18 @@
         )
         return values * cosines + partner * sines
 
-    weight_copies[0].wait()
+    with jax.named_scope("wait_k"):
+        weight_copies[0].wait()
     keys = rotated(rounded(key_w)) * head_width ** (-0.5)
-    weight_copies[1].wait()
+    with jax.named_scope("wait_q"):
+        weight_copies[1].wait()
     queries = rotated(rounded(query_w))
     for block in range(blocks):
         span = slice(block * BLOCK, (block + 1) * BLOCK)
         key_columns[block] = keys[span].T
         query_columns[block] = queries[span].T
-    weight_copies[2].wait()
+    with jax.named_scope("wait_v"):
+        weight_copies[2].wait()
     values = rounded(value_w)
     for head in range(heads):
         value_heads[head] = values[:, head * head_width : (head + 1) * head_width]
@@ -317,33 +378,61 @@
         jnp.exp(jnp.full((1, head_width), -decay_rate[head], jnp.float32)) for head in range(heads)
     ]
 
+    products = keys * queries
+    for head in range(heads):
+        span = slice(head * head_width, (head + 1) * head_width)
+        overlap[head] = jnp.sum(products[:, span], axis=1, keepdims=True)
+
+    def read(block, carry):
+        state_in(block).wait()
+        span = pl.ds(block * BLOCK, BLOCK)
+        for head in range(heads):
+            lanes = slice(head * head_width, (head + 1) * head_width)
+            block_queries = query_columns[block, lanes, :]
+            read_rows = [
+                jnp.sum(
+                    block_queries[:, index : index + 1] * state[block * BLOCK + index, head],
+                    axis=0,
+                    keepdims=True,
+                )
+                for index in range(BLOCK)
+            ]
+            reading[head, span, :] = (
+                retain[head] * jnp.concatenate(read_rows, axis=0)
+                + overlap[head, span, :] * value_heads[head, span, :]
+            )
+        return carry
+
     def update(block, carry):
-        state_in(block).wait()
+        span = pl.ds(block * BLOCK, BLOCK)
         for head in range(heads):
-            span = slice(head * head_width, (head + 1) * head_width)
-            block_values = value_heads[head, pl.ds(block * BLOCK, BLOCK), :]
-            block_keys = key_columns[block, span, :]
-            block_queries = query_columns[block, span, :]
-            read_rows = []
+            lanes = slice(head * head_width, (head + 1) * head_width)
+            block_values = value_heads[head, span, :]
+            block_keys = key_columns[block, lanes, :]
             for index in range(BLOCK):
                 sequence = block * BLOCK + index
-                fresh = (
+                state[sequence, head] = (
                     retain[head] * state[sequence, head]
                     + block_keys[:, index : index + 1] * block_values[index : index + 1, :]
                 )
-                state[sequence, head] = fresh
-                read_rows.append(
-                    jnp.sum(block_queries[:, index : index + 1] * fresh, axis=0, keepdims=True)
-                )
-            reading[head, pl.ds(block * BLOCK, BLOCK), :] = jnp.concatenate(read_rows, axis=0)
         return carry
 
-    lax.fori_loop(0, blocks // 2, update, 0)
-    spread_tokens(1)
-    lax.fori_loop(blocks // 2, blocks, update, 0)
-    weight_copies[3].wait()
+    def advance(first, last):
+        with jax.named_scope(f"advance_{first}"):
+            lax.fori_loop(first, last, update, 0)
+
+    with jax.named_scope("read_a"):
+        lax.fori_loop(0, 2 * blocks // 3, read, 0)
+    with jax.named_scope("spread_tokens_2"):
+        spread_tokens(2)
+    with jax.named_scope("read_b"):
+        lax.fori_loop(2 * blocks // 3, blocks, read, 0)
+    with jax.named_scope("spread_tokens_1"):
+        spread_tokens(1)
+    with jax.named_scope("wait_g"):
+        weight_copies[3].wait()
     gating = rounded(gate_w)
-    read = jnp.concatenate(
+    read_heads = jnp.concatenate(
         [
             rms(
                 reading[head],
@@ -353,58 +442,66 @@
         ],
         axis=1,
     )
-    mixed_heads = (read * jax.nn.silu(gating)).astype(jnp.bfloat16)
+    mixed_heads = (read_heads * jax.nn.silu(gating)).astype(jnp.bfloat16)
     hsend[...] = dot(placing, mixed_heads).astype(jnp.bfloat16).reshape(hsend.shape)
     each_column(lambda step: column_copy(hsend, hrecv, h_sems, step).start())
     hrecv[0] = hsend[group]
-    spread_heads(0)
-    spread_tokens(2)
-    spread_tokens(3)
-    weight_copies[4].wait()
-    mixed = (inputs + dot(mixed_heads, out_w[...])).astype(jnp.bfloat16)
-    for stage in range(1, STAGES):
-        spread_heads(stage)
-    for load in loads:
-        load.wait()
+    with jax.named_scope("spread_heads_0"):
+        spread_heads(0)
+    with jax.named_scope("spread_tokens_3"):
+        spread_tokens(3)
+    for stage in ORDER:
+        with jax.named_scope(f"spread_heads_{stage}"):
+            spread_heads(stage)
+    with jax.named_scope("wait_oe"):
+        weight_copies[4].wait()
+        for load in loads:
+            load.wait()
 
     def run_expert(stage):
-        each_plane(lambda step: plane_copy(dsend, drecv, d_sems, stage, step).wait_recv())
-        each_plane(lambda step: plane_copy(esend, erecv, e_sems, stage, step).wait_recv())
-        token_rows = drecv[stage].reshape(rows, width).astype(jnp.float32)
-        head_rows = erecv[stage].reshape(rows, erecv.shape[-1])
+        plane_total(dsend, drecv, d_sems, stage).wait_recv()
+        plane_total(esend, erecv, e_sems, stage).wait_recv()
+        token_rows = unstacked(dot(packing, load_packed(drecv, stage)))
+        head_rows = unstacked(dot(packing, load_packed(erecv, stage))).astype(jnp.bfloat16)
         block = (token_rows + dot(head_rows, out_w[...])).astype(jnp.bfloat16)
         block = rms(block.astype(jnp.float32), moe_gain[...]).astype(jnp.bfloat16)
         hidden = jax.nn.silu(dot(block, expert_gate_w[...])) * dot(block, expert_up_w[...])
         block = dot(hidden.astype(jnp.bfloat16), expert_down_w[...]).astype(jnp.bfloat16)
-        osend[stage] = block.reshape(osend.shape[1:])
+        store_packed(osend, stage, take(packing, stacked(block)))
 
     def send_back(stage):
         each_plane(lambda step: plane_copy(osend, orecv, o_sems, stage, step).start())
         orecv[stage, inner] = osend[stage, inner]
 
     def combine(stage):
-        each_plane(lambda step: plane_copy(osend, orecv, o_sems, stage, step).wait_recv())
-        block = orecv[stage].reshape(rows, width)
+        plane_total(osend, orecv, o_sems, stage).wait_recv()
+        block = load_packed(orecv, stage)
         high, low = weights_of[stage]
-        csend[stage] = (dot(high, block) + dot(low, block)).astype(jnp.bfloat16)
+        csend[stage] = unstacked(dot(high, block) + dot(low, block)).astype(jnp.bfloat16)
         if stage:
             send_home(stage).start()
         else:
             crecv[group] = csend[0]
 
-    run_expert(0)
-    run_expert(1)
-    send_back(1)
-    run_expert(2)
-    send_back(2)
-    run_expert(3)
-    send_back(3)
+    advance(0, blocks // 6)
+    with jax.named_scope("run_expert_0"):
+        run_expert(0)
+    for stage in ORDER:
+        with jax.named_scope(f"run_expert_{stage}"):
+            run_expert(stage)
+        send_back(stage)
     send_back(0)
-    combine(1)
-    combine(2)
-    combine(3)
-    combine(0)
-    each_column(lambda step: send_home(step).wait_recv())
+    advance(blocks // 6, blocks // 2)
+    for place, stage in enumerate(ORDER):
+        with jax.named_scope(f"combine_{stage}"):
+            combine(stage)
+        advance((3 + place) * blocks // 6, (4 + place) * blocks // 6)
+    with jax.named_scope("combine_0"):
+        combine(0)
+    with jax.named_scope("mixed"):
+        mixed = (inputs + dot(mixed_heads, out_w[...])).astype(jnp.bfloat16)
+    with jax.named_scope("wait_home"):
+        each_column(lambda step: send_home(step).wait_recv())
     block = dot(collecting, crecv[...].reshape(slots, width))
     out[...] = (mixed.astype(jnp.float32) + block).astype(jnp.bfloat16)
     each_column(lambda step: column_copy(meta_send, meta_recv, meta_sems, step).wait_send())
@@ -412,13 +509,40 @@
     each_column(lambda step: column_copy(hsend, hrecv, h_sems, step).wait_send())
     each_column(lambda step: send_home(step).wait_send())
 
-    def drain(stage, carry):
-        each_plane(lambda step: plane_copy(dsend, drecv, d_sems, stage, step).wait_send())
-        each_plane(lambda step: plane_copy(esend, erecv, e_sems, stage, step).wait_send())
-        each_plane(lambda step: plane_copy(osend, orecv, o_sems, stage, step).wait_send())
-        return carry
-
-    lax.fori_loop(0, STAGES, drain, 0)
+    for stage in range(STAGES):
+        plane_total(dsend, drecv, d_sems, stage).wait_send()
+        plane_total(esend, erecv, e_sems, stage).wait_send()
+        plane_total(osend, orecv, o_sems, stage).wait_send()
+
+
+def finish_kernel(output, state, out, state_out, sem):
+    blocks = sem.shape[0] - 1
+    share = state.shape[0] // blocks
+    copies = [pltpu.make_async_copy(output, out, sem.at[blocks])]
+    for block in range(blocks):
+        span = pl.ds(block * share, share)
+        copies.append(pltpu.make_async_copy(state.at[span], state_out.at[span], sem.at[block]))
+    for copy in copies:
+        copy.start()
+    for copy in copies:
+        copy.wait()
+
+
+def finish(output, new_state):
+    vmem = pl.BlockSpec(memory_space=pltpu.VMEM)
+    hbm = pl.BlockSpec(memory_space=pl.ANY)
+    return pl.pallas_call(
+        finish_kernel,
+        name="finish",
+        out_shape=(
+            jax.ShapeDtypeStruct(output.shape, output.dtype),
+            jax.ShapeDtypeStruct(new_state.shape, new_state.dtype),
+        ),
+        in_specs=[vmem, vmem],
+        out_specs=(hbm, hbm),
+        scratch_shapes=[pltpu.SemaphoreType.DMA((2 * new_state.shape[0] // BLOCK + 1,))],
+        compiler_params=pltpu.CompilerParams(vmem_limit_bytes=4 * 1024 * 1024),
+    )(output, new_state)
 
 
 def local(
@@ -452,7 +576,8 @@
     inverse = (10000.0 ** (-np.arange(half) / half)).astype(np.float32)
     capacity = max(2, 4 * seq_count // experts)
     group_rows = -(-min(seq_count, per_group * capacity // TOP_K) // 8) * 8
-    peer_rows = -(-capacity // 8) * 8
+    capacity += capacity % 2
+    packed = capacity * QUARTERS // BLOCK
     vmem = pl.BlockSpec(memory_space=pltpu.VMEM)
     smem = pl.BlockSpec(memory_space=pltpu.SMEM)
     hbm = pl.BlockSpec(memory_space=pl.ANY)
@@ -463,19 +588,19 @@
         return [pltpu.VMEM((GROUPS, group_rows, lanes), bf16)] * 2
 
     def plane_buffer(lanes):
-        return [pltpu.VMEM((STAGES, per_group, peer_rows, lanes), bf16)] * 2
+        return [pltpu.VMEM((STAGES, per_group, BLOCK, lanes * packed // QUARTERS), bf16)] * 2
 
     weights = (w_query, w_key, w_value, w_gate, w_out, expert_gate[0], expert_up[0], expert_down[0])
     state_bytes = state.size // head_width * max(head_width, 128) * 4
 
     def kernel(*refs):
-        layer_kernel(per_group, *refs)
+        layer_kernel(per_group, capacity, *refs)
 
     output, new_state = pl.pallas_call(
         kernel,
         name="layer",
         out_shape=(
-            jax.ShapeDtypeStruct((seq_count, model_width), bf16),
+            pltpu.VMEM((seq_count, model_width), bf16),
             pltpu.VMEM(state.shape, f32),
         ),
         in_specs=[vmem] * 4 + [smem] + [vmem] * 5 + [hbm] * 9,
@@ -486,6 +611,7 @@
             pltpu.VMEM((blocks, mixed_width, BLOCK), f32),
             pltpu.VMEM((heads, seq_count, head_width), f32),
             pltpu.VMEM((heads, seq_count, head_width), f32),
+            pltpu.VMEM((heads, seq_count, 1), f32),
         ]
         + column_buffer(128)
         + column_buffer(model_width)
@@ -501,9 +627,9 @@
             dma((2, GROUPS)),
             dma((2, GROUPS)),
             dma((2, GROUPS)),
-            dma((2, STAGES, per_group)),
-            dma((2, STAGES, per_group)),
-            dma((2, STAGES, per_group)),
+            dma((2, STAGES)),
+            dma((2, STAGES)),
+            dma((2, STAGES)),
             dma((2, STAGES)),
         ],
         compiler_params=pltpu.CompilerParams(
@@ -532,7 +658,7 @@
         expert_up[0],
         expert_down[0],
     )
-    return (output, new_state)
+    return finish(output, new_state)
 
 
 def solution(mesh):

time: 55.7 us -> 48.4 us (0.87)
  local copies, waits for them, and re-layouts: 5.46 us -> 0 us
  Pallas kernels: 49.1 us -> 47.4 us
    unnamed x4 -> x0, local copies, waits for them, and re-layouts: 5.46 us -> none
    pallas_call x1 -> x2, Pallas kernels: 49.1 us -> 47.4 us  [the longest x1 42.7 us: local(): pl.pallas_call(kernel, name='layer', out_shape=(pltpu.VMEM((seq_count, mo...]
where the time goes in v2:
time: 48.4 us; the launch traced here: 48.2 us
  Pallas kernels  47.4 us (98%)
  between operations  0.81 us (2%)
    pallas_call x1, Pallas kernels, local(): pl.pallas_call(kernel, name='layer', out_shape=(pltpu.VMEM((seq_count, mo...  42.7 us
    pallas_call x1, Pallas kernels, finish(): pl.pallas_call(finish_kernel, name='finish', out_shape=(jax.ShapeDtypeStr...  4.74 us

profile of v2, /device:TPU:0, one launch (start us, length us, event | category | flops | bytes accessed | tf_op | source)
XLA Modules:
  0.0 48.2 jit_solution(3198401626611633003)
XLA Ops:
  0.6 42.7 %layer.1 = (bf16[48,2048]{1,0:T(8,128)(2,1)S(1)}, f32[48,8,64,64]{3,2,1,0:T(8,128)S(1)}) custom-call(bf16[48,2048]{1,0:T(8,128)(2,1)} %refs_0_.1, s32[1,48]{1,0:T(1,128)} %bitcast.18, f32[1,32]{1,0:T(1,128)} %constant.2.clone.refs_2_, f32[1,2048]{1,0:T(1,128)} %bitcast.13, f32[8]{0:T(128)} %refs_4_.1, f32[1,512]{1,0:T(1,128)} %bitcast.15, ...), custom_call_target="tpu_custom_call" | custom-call | tf_op jit(solution)/shard_map/layer/pallas_call | solution.py:599
  43.3 4.7 %finish.1 = (bf16[48,2048]{1,0:T(8,128)(2,1)}, f32[48,8,64,64]{3,2,1,0:T(8,128)}) custom-call(bf16[48,2048]{1,0:T(8,128)(2,1)S(1)} %get-tuple-element.4.output, f32[48,8,64,64]{3,2,1,0:T(8,128)S(1)} %get-tuple-element.5.state), custom_call_target="tpu_custom_call" | custom-call | tf_op jit(solution)/shard_map/finish/pallas_call | solution.py:534

commit v3 on v2

--- a/solution.py
+++ b/solution.py
@@ -34,16 +34,16 @@
 def layer_kernel(
     per_group,
     capacity,
-    tokens,
-    history_length,
-    inverse,
-    norm_gain,
     decay_rate,
-    head_gain,
-    moe_gain,
-    expert_group,
-    expert_inner,
-    route_weights,
+    tokens_hbm,
+    history_length_hbm,
+    inverse_hbm,
+    norm_gain_hbm,
+    head_gain_hbm,
+    moe_gain_hbm,
+    expert_group_hbm,
+    expert_inner_hbm,
+    route_weights_hbm,
     query_hbm,
     key_hbm,
     value_hbm,
@@ -63,8 +63,17 @@
     expert_gate_w,
     expert_up_w,
     expert_down_w,
-    query_columns,
+    tokens,
+    history_length,
+    inverse,
+    norm_gain,
+    head_gain,
+    moe_gain,
+    expert_group,
+    expert_inner,
+    route_weights,
     key_columns,
+    query_heads,
     value_heads,
     reading,
     overlap,
@@ -82,6 +91,7 @@
     orecv,
     csend,
     crecv,
+    small_sem,
     weight_sem,
     in_sem,
     load_sem,
@@ -107,7 +117,7 @@
     blocks = seq_count // BLOCK
 
     def column_peer(step):
-        other = lax.rem(group + step, GROUPS)
+        other = {1: group + 1 - 2 * (group % 2), 2: (group + 2) % GROUPS, 3: GROUPS - 1 - group}[step]
         return other, other * per_group + inner
 
     def plane_peer(step):
@@ -129,13 +139,12 @@
         return remote(source.at[other], target.at[step], sems.at[0, step], sems.at[1, step], peer)
 
     def send_home(step):
-        home = lax.rem(group + GROUPS - step, GROUPS)
         return remote(
             csend.at[step],
             crecv.at[group],
             c_sems.at[0, step],
             c_sems.at[1, step],
-            home * per_group + inner,
+            column_peer(step)[1],
         )
 
     def plane_copy(source, target, sems, stage, step):
@@ -175,10 +184,32 @@
             for index, (source, target) in enumerate(pairs)
         ]
 
+    barrier = pltpu.get_barrier_semaphore()
+
+    def greet_column(step):
+        pl.semaphore_signal(barrier, inc=1, device_id=(column_peer(step)[1],), device_id_type=MESH)
+
+    def greet_plane(step):
+        pl.semaphore_signal(barrier, inc=1, device_id=(plane_peer(step)[1],), device_id_type=MESH)
+
+    smalls = load_all(
+        (
+            (expert_group_hbm, expert_group),
+            (tokens_hbm, tokens),
+            (expert_inner_hbm, expert_inner),
+            (route_weights_hbm, route_weights),
+            (norm_gain_hbm, norm_gain),
+            (history_length_hbm, history_length),
+            (inverse_hbm, inverse),
+            (head_gain_hbm, head_gain),
+            (moe_gain_hbm, moe_gain),
+        ),
+        small_sem,
+    )
     weight_copies = load_all(
         (
+            (query_hbm, query_w),
             (key_hbm, key_w),
-            (query_hbm, query_w),
             (value_hbm, value_w),
             (gate_hbm, gate_w),
             (out_hbm, out_w),
@@ -198,25 +229,12 @@
         span = pl.ds(block * BLOCK, BLOCK)
         return pltpu.make_async_copy(state_hbm.at[span], state.at[span], in_sem.at[block])
 
-    for copy in weight_copies[:3]:
+    for copy in smalls + weight_copies[:1]:
         copy.start()
-    for block in range(blocks):
-        state_in(block).start()
-    for copy in weight_copies[3:]:
-        copy.start()
-    for load in loads:
-        load.start()
-
-    barrier = pltpu.get_barrier_semaphore()
-
-    def greet_column(step):
-        pl.semaphore_signal(barrier, inc=1, device_id=(column_peer(step)[1],), device_id_type=MESH)
-
-    def greet_plane(step):
-        pl.semaphore_signal(barrier, inc=1, device_id=(plane_peer(step)[1],), device_id_type=MESH)
-
     each_column(greet_column)
     each_plane(greet_plane)
+    for copy in weight_copies[1:3]:
+        copy.start()
 
     square = (seq_count, seq_count)
     above = lax.broadcasted_iota(jnp.int32, square, 0)
@@ -229,9 +247,20 @@
         matched = sum((values == row).astype(jnp.float32) for values in columns)
         return jnp.sum(jnp.where(above < across, matched, 0.0), axis=0, keepdims=True)
 
+    smalls[0].wait()
     group_row = expert_group[...].astype(jnp.float32)
+    group_slot = group_row * group_rows + earlier([column(group_row)], group_row)
+    slot_above = lax.broadcasted_iota(jnp.int32, (slots, seq_count), 0).astype(jnp.float32)
+    placing = (slot_above == group_slot).astype(jnp.float32).astype(jnp.bfloat16)
+    smalls[1].wait()
+    zsend[...] = dot(placing, tokens[...]).astype(jnp.bfloat16).reshape(zsend.shape)
+    with jax.named_scope("barrier"):
+        pl.semaphore_wait(barrier, GROUPS - 1 + per_group - 1)
+    for stage in (1, 2):
+        column_copy(zsend, zrecv, z_sems, stage).start()
+    for small in smalls[2:4]:
+        small.wait()
     inner_rows = [expert_inner[choice : choice + 1, :].astype(jnp.float32) for choice in (0, 1)]
-    group_slot = group_row * group_rows + earlier([column(group_row)], group_row)
     expert_rows = [group_row * per_group + row for row in inner_rows]
     expert_columns = [column(row) for row in expert_rows]
     lanes = []
@@ -246,19 +275,12 @@
     token_meta = jnp.zeros(lane.shape, jnp.float32)
     for index, value in enumerate(lanes):
         token_meta = jnp.where(lane == index, value, token_meta)
-    slot_above = lax.broadcasted_iota(jnp.int32, (slots, seq_count), 0).astype(jnp.float32)
-    slot_across = lax.broadcasted_iota(jnp.int32, (seq_count, slots), 1).astype(jnp.float32)
-    placing = (slot_above == group_slot).astype(jnp.float32).astype(jnp.bfloat16)
-    collecting = (slot_across == column(group_slot)).astype(jnp.float32).astype(jnp.bfloat16)
     meta = dot(placing, token_meta.astype(jnp.bfloat16)).astype(jnp.bfloat16)
     meta_send[...] = meta.reshape(meta_send.shape)
-    zsend[...] = dot(placing, tokens[...]).astype(jnp.bfloat16).reshape(zsend.shape)
-    with jax.named_scope("barrier"):
-        pl.semaphore_wait(barrier, GROUPS - 1 + per_group - 1)
     each_column(lambda step: column_copy(meta_send, meta_recv, meta_sems, step).start())
-    each_column(lambda step: column_copy(zsend, zrecv, z_sems, step).start())
     meta_recv[0] = meta_send[group]
     zrecv[0] = zsend[group]
+
     def packed_places(shape, axis):
         index = lax.broadcasted_iota(jnp.int32, shape, axis)
         part = sum((index >= tiles * bound).astype(jnp.int32) for bound in range(1, parts))
@@ -337,9 +359,8 @@
             column_copy(hsend, hrecv, h_sems, stage).wait_recv()
         spread(stage, hrecv, esend, erecv, e_sems)
 
-    with jax.named_scope("spread_tokens_0"):
-        spread_tokens(0)
-
+    for small in smalls[4:]:
+        small.wait()
     inputs = tokens[...].astype(jnp.float32)
     normed = rms(inputs, norm_gain[...]).astype(jnp.bfloat16)
     places = column(history_length[...].astype(jnp.float32))
@@ -359,46 +380,48 @@
         )
         return values * cosines + partner * sines
 
+    def head_lanes(head):
+        return slice(head * head_width, (head + 1) * head_width)
+
+    with jax.named_scope("wait_q"):
+        weight_copies[0].wait()
+    queries = rotated(rounded(query_w))
+    for head in range(heads):
+        query_heads[head] = queries[:, head_lanes(head)]
+    for block in range(blocks):
+        if block == blocks - 2:
+            weight_copies[3].start()
+        state_in(block).start()
     with jax.named_scope("wait_k"):
-        weight_copies[0].wait()
+        weight_copies[1].wait()
     keys = rotated(rounded(key_w)) * head_width ** (-0.5)
-    with jax.named_scope("wait_q"):
-        weight_copies[1].wait()
-    queries = rotated(rounded(query_w))
-    for block in range(blocks):
-        span = slice(block * BLOCK, (block + 1) * BLOCK)
-        key_columns[block] = keys[span].T
-        query_columns[block] = queries[span].T
     with jax.named_scope("wait_v"):
         weight_copies[2].wait()
     values = rounded(value_w)
+    products = keys * queries
     for head in range(heads):
-        value_heads[head] = values[:, head * head_width : (head + 1) * head_width]
+        value_heads[head] = values[:, head_lanes(head)]
+        overlap[head] = jnp.sum(products[:, head_lanes(head)], axis=1, keepdims=True)
     retain = [
         jnp.exp(jnp.full((1, head_width), -decay_rate[head], jnp.float32)) for head in range(heads)
     ]
-
-    products = keys * queries
-    for head in range(heads):
-        span = slice(head * head_width, (head + 1) * head_width)
-        overlap[head] = jnp.sum(products[:, span], axis=1, keepdims=True)
+    wide = (BLOCK, BLOCK * head_width)
+    own = lax.broadcasted_iota(jnp.int32, wide, 0) == (
+        lax.broadcasted_iota(jnp.int32, wide, 1) // head_width
+    )
 
     def read(block, carry):
         state_in(block).wait()
         span = pl.ds(block * BLOCK, BLOCK)
         for head in range(heads):
-            lanes = slice(head * head_width, (head + 1) * head_width)
-            block_queries = query_columns[block, lanes, :]
-            read_rows = [
-                jnp.sum(
-                    block_queries[:, index : index + 1] * state[block * BLOCK + index, head],
-                    axis=0,
-                    keepdims=True,
-                )
-                for index in range(BLOCK)
-            ]
+            block_queries = query_heads[head, span, :]
+            spread_queries = jnp.where(own, jnp.concatenate([block_queries] * BLOCK, axis=1), 0.0)
+            high = spread_queries.astype(jnp.bfloat16).astype(jnp.float32)
+            both = jnp.concatenate([high, spread_queries - high], axis=0).astype(jnp.bfloat16)
+            old = state[span, head].reshape(BLOCK * head_width, head_width).astype(jnp.bfloat16)
+            found = dot(both, old)
             reading[head, span, :] = (
-                retain[head] * jnp.concatenate(read_rows, axis=0)
+                retain[head] * (found[:BLOCK] + found[BLOCK:])
                 + overlap[head, span, :] * value_heads[head, span, :]
             )
         return carry
@@ -421,14 +444,17 @@
         with jax.named_scope(f"advance_{first}"):
             lax.fori_loop(first, last, update, 0)
 
+    with jax.named_scope("spread_tokens_0"):
+        spread_tokens(0)
+    column_copy(zsend, zrecv, z_sems, 3).start()
     with jax.named_scope("read_a"):
-        lax.fori_loop(0, 2 * blocks // 3, read, 0)
-    with jax.named_scope("spread_tokens_2"):
-        spread_tokens(2)
-    with jax.named_scope("read_b"):
-        lax.fori_loop(2 * blocks // 3, blocks, read, 0)
+        lax.fori_loop(0, blocks // 2, read, 0)
     with jax.named_scope("spread_tokens_1"):
         spread_tokens(1)
+    with jax.named_scope("read"):
+        lax.fori_loop(blocks // 2, blocks, read, 0)
+    for copy in weight_copies[4:] + loads:
+        copy.start()
     with jax.named_scope("wait_g"):
         weight_copies[3].wait()
     gating = rounded(gate_w)
@@ -436,7 +462,7 @@
         [
             rms(
                 reading[head],
-                head_gain[:, head * head_width : (head + 1) * head_width],
+                head_gain[:, head_lanes(head)],
             )
             for head in range(heads)
         ],
@@ -446,17 +472,19 @@
     hsend[...] = dot(placing, mixed_heads).astype(jnp.bfloat16).reshape(hsend.shape)
     each_column(lambda step: column_copy(hsend, hrecv, h_sems, step).start())
     hrecv[0] = hsend[group]
+    for block in range(blocks):
+        key_columns[block] = keys[block * BLOCK : (block + 1) * BLOCK].T
     with jax.named_scope("spread_heads_0"):
         spread_heads(0)
-    with jax.named_scope("spread_tokens_3"):
-        spread_tokens(3)
-    for stage in ORDER:
+    advance(0, blocks // 6)
+    with jax.named_scope("spread_tokens_2"):
+        spread_tokens(2)
+    for stage in ORDER[:2]:
         with jax.named_scope(f"spread_heads_{stage}"):
             spread_heads(stage)
     with jax.named_scope("wait_oe"):
-        weight_copies[4].wait()
-        for load in loads:
-            load.wait()
+        for copy in weight_copies[4:] + loads:
+            copy.wait()
 
     def run_expert(stage):
         plane_total(dsend, drecv, d_sems, stage).wait_recv()
@@ -483,25 +511,39 @@
         else:
             crecv[group] = csend[0]
 
-    advance(0, blocks // 6)
+    advance(blocks // 6, 3 * blocks // 6)
+    with jax.named_scope("spread_tokens_3"):
+        spread_tokens(3)
+    with jax.named_scope("spread_heads_3"):
+        spread_heads(3)
+    with jax.named_scope("run_expert_2"):
+        run_expert(2)
+    send_back(2)
+    with jax.named_scope("run_expert_1"):
+        run_expert(1)
+    with jax.named_scope("run_expert_3"):
+        run_expert(3)
+    send_back(3)
+    with jax.named_scope("combine_2"):
+        combine(2)
+    send_back(1)
     with jax.named_scope("run_expert_0"):
         run_expert(0)
-    for stage in ORDER:
-        with jax.named_scope(f"run_expert_{stage}"):
-            run_expert(stage)
-        send_back(stage)
     send_back(0)
-    advance(blocks // 6, blocks // 2)
-    for place, stage in enumerate(ORDER):
-        with jax.named_scope(f"combine_{stage}"):
-            combine(stage)
-        advance((3 + place) * blocks // 6, (4 + place) * blocks // 6)
+    with jax.named_scope("combine_3"):
+        combine(3)
+    advance(3 * blocks // 6, 4 * blocks // 6)
+    with jax.named_scope("combine_1"):
+        combine(1)
+    advance(4 * blocks // 6, blocks)
     with jax.named_scope("combine_0"):
         combine(0)
     with jax.named_scope("mixed"):
         mixed = (inputs + dot(mixed_heads, out_w[...])).astype(jnp.bfloat16)
     with jax.named_scope("wait_home"):
         each_column(lambda step: send_home(step).wait_recv())
+    slot_across = lax.broadcasted_iota(jnp.int32, (seq_count, slots), 1).astype(jnp.float32)
+    collecting = (slot_across == column(group_slot)).astype(jnp.float32).astype(jnp.bfloat16)
     block = dot(collecting, crecv[...].reshape(slots, width))
     out[...] = (mixed.astype(jnp.float32) + block).astype(jnp.bfloat16)
     each_column(lambda step: column_copy(meta_send, meta_recv, meta_sems, step).wait_send())
@@ -593,6 +635,18 @@
     weights = (w_query, w_key, w_value, w_gate, w_out, expert_gate[0], expert_up[0], expert_down[0])
     state_bytes = state.size // head_width * max(head_width, 128) * 4
 
+    smalls = (
+        tokens,
+        history_length.reshape(1, -1),
+        inverse.reshape(1, -1),
+        norm_gain.reshape(1, -1),
+        head_gain.reshape(1, -1),
+        moe_gain.reshape(1, -1),
+        expert_group.reshape(1, -1),
+        expert_inner.T,
+        route_weights.T,
+    )
+
     def kernel(*refs):
         layer_kernel(per_group, capacity, *refs)
 
@@ -603,12 +657,13 @@
             pltpu.VMEM((seq_count, model_width), bf16),
             pltpu.VMEM(state.shape, f32),
         ),
-        in_specs=[vmem] * 4 + [smem] + [vmem] * 5 + [hbm] * 9,
+        in_specs=[smem] + [hbm] * 18,
         out_specs=(vmem, vmem),
         scratch_shapes=[pltpu.VMEM(weight.shape, bf16) for weight in weights]
+        + [pltpu.VMEM(small.shape, small.dtype) for small in smalls]
         + [
             pltpu.VMEM((blocks, mixed_width, BLOCK), f32),
-            pltpu.VMEM((blocks, mixed_width, BLOCK), f32),
+            pltpu.VMEM((heads, seq_count, head_width), f32),
             pltpu.VMEM((heads, seq_count, head_width), f32),
             pltpu.VMEM((heads, seq_count, head_width), f32),
             pltpu.VMEM((heads, seq_count, 1), f32),
@@ -621,6 +676,7 @@
         + plane_buffer(model_width)
         + column_buffer(model_width)
         + [
+            dma((9,)),
             dma((5,)),
             dma((blocks,)),
             dma((3,)),
@@ -638,16 +694,8 @@
             vmem_limit_bytes=63 * 1024 * 1024 - state_bytes,
         ),
     )(
-        tokens,
-        history_length.reshape(1, -1),
-        inverse.reshape(1, -1),
-        norm_gain.reshape(1, -1),
         decay_rate,
-        head_gain.reshape(1, -1),
-        moe_gain.reshape(1, -1),
-        expert_group.reshape(1, -1),
-        expert_inner.T,
-        route_weights.T,
+        *smalls,
         w_query,
         w_key,
         w_value,

time: 48.4 us -> 45.8 us (0.946)
  Pallas kernels: 47.4 us -> 45 us
    pallas_call x1, Pallas kernels: 42.7 us -> 40.2 us  [local(): pl.pallas_call(kernel, name='layer', out_shape=(pltpu.VMEM((seq_count, mo...]
where the time goes in v3:
time: 45.8 us; the launch traced here: 45.6 us
  Pallas kernels  45 us (98%)
  between operations  0.65 us (1%)
    pallas_call x1, Pallas kernels, local(): pl.pallas_call(kernel, name='layer', out_shape=(pltpu.VMEM((seq_count, mo...  40.2 us
    pallas_call x1, Pallas kernels, finish(): pl.pallas_call(finish_kernel, name='finish', out_shape=(jax.ShapeDtypeStr...  4.74 us

profile of v3, /device:TPU:0, one launch (start us, length us, event | category | flops | bytes accessed | tf_op | source)
XLA Modules:
  0.0 45.6 jit_solution(3369455021855117776)
XLA Ops:
  0.6 40.2 %layer.1 = (bf16[48,2048]{1,0:T(8,128)(2,1)S(1)}, f32[48,8,64,64]{3,2,1,0:T(8,128)S(1)}) custom-call(f32[8]{0:T(128)} %refs_0_.1, bf16[48,2048]{1,0:T(8,128)(2,1)} %refs_1_.1, s32[1,48]{1,0:T(1,128)} %bitcast.18, f32[1,32]{1,0:T(1,128)} %constant.2.clone.refs_3_, f32[1,2048]{1,0:T(1,128)} %bitcast.13, f32[1,512]{1,0:T(1,128)} %bitcast.15, ...), custom_call_target="tpu_custom_call" | custom-call | tf_op jit(solution)/shard_map/layer/pallas_call | solution.py:653
  40.9 4.7 %finish.1 = (bf16[48,2048]{1,0:T(8,128)(2,1)}, f32[48,8,64,64]{3,2,1,0:T(8,128)}) custom-call(bf16[48,2048]{1,0:T(8,128)(2,1)S(1)} %get-tuple-element.4.output, f32[48,8,64,64]{3,2,1,0:T(8,128)S(1)} %get-tuple-element.5.state), custom_call_target="tpu_custom_call" | custom-call | tf_op jit(solution)/shard_map/finish/pallas_call | solution.py:576

commit v4 on v3

--- a/solution.py
+++ b/solution.py
@@ -19,7 +19,8 @@
 MESH = pl.DeviceIdType.MESH
 STAGES = GROUPS
 QUARTERS = 4
-ORDER = (2, 1, 3)
+HALVES = 2
+ORDER = (2, 3, 1)
 
 
 def dot(a, b):
@@ -73,8 +74,8 @@
     expert_inner,
     route_weights,
     key_columns,
+    value_heads,
     query_heads,
-    value_heads,
     reading,
     overlap,
     meta_send,
@@ -136,14 +137,19 @@
 
     def column_copy(source, target, sems, step):
         other, peer = column_peer(step)
-        return remote(source.at[other], target.at[step], sems.at[0, step], sems.at[1, step], peer)
-
-    def send_home(step):
+        return remote(source.at[other], target.at[step], sems.at[0], sems.at[step], peer)
+
+    def column_sent(source, target, sems):
+        others = pl.ds(1, GROUPS - 1)
+        return remote(source.at[others], target.at[others], sems.at[0], sems.at[1], column_peer(1)[1])
+
+    def send_home(step, half):
+        index = step * HALVES + half
         return remote(
-            csend.at[step],
-            crecv.at[group],
-            c_sems.at[0, step],
-            c_sems.at[1, step],
+            csend.at[step, half],
+            crecv.at[group, half],
+            c_sems.at[0],
+            c_sems.at[index],
             column_peer(step)[1],
         )
 
@@ -152,8 +158,8 @@
         return remote(
             source.at[stage, other],
             target.at[stage, inner],
-            sems.at[0, stage],
-            sems.at[1, stage],
+            sems.at[0],
+            sems.at[stage + 1],
             peer,
         )
 
@@ -162,9 +168,15 @@
         return remote(
             source.at[stage, others],
             target.at[stage, others],
-            sems.at[0, stage],
-            sems.at[1, stage],
+            sems.at[0],
+            sems.at[stage + 1],
             plane_peer(1)[1],
+        )
+
+    def plane_sent(source, target, sems):
+        others = pl.ds(0, per_group - 1)
+        return remote(
+            source.at[:, others], target.at[:, others], sems.at[0], sems.at[1], plane_peer(1)[1]
         )
 
     def each_column(act):
@@ -256,8 +268,17 @@
     zsend[...] = dot(placing, tokens[...]).astype(jnp.bfloat16).reshape(zsend.shape)
     with jax.named_scope("barrier"):
         pl.semaphore_wait(barrier, GROUPS - 1 + per_group - 1)
-    for stage in (1, 2):
-        column_copy(zsend, zrecv, z_sems, stage).start()
+    outer = group * (GROUPS - 1 - group) == 0
+
+    def send_tokens(stage, held):
+        @pl.when(outer if held else jnp.logical_not(outer))
+        def start():
+            column_copy(zsend, zrecv, z_sems, stage).start()
+
+    send_tokens(2, True)
+    send_tokens(1, False)
+    for block in range(2):
+        state_in(block).start()
     for small in smalls[2:4]:
         small.wait()
     inner_rows = [expert_inner[choice : choice + 1, :].astype(jnp.float32) for choice in (0, 1)]
@@ -342,9 +363,9 @@
         picks_of[stage] = picks.astype(jnp.bfloat16)
         weights_of[stage] = (high, (weights - high.astype(jnp.float32)).astype(jnp.bfloat16))
 
-    def spread(stage, received, sent, landed, sems):
+    def spread(stage, picks, received, sent, landed, sems):
         block = stacked(received[stage].astype(jnp.float32)).astype(jnp.bfloat16)
-        store_packed(sent, stage, take(picks_of[stage], block))
+        store_packed(sent, stage, take(picks, block))
         each_plane(lambda step: plane_copy(sent, landed, sems, stage, step).start())
         landed[stage, inner] = sent[stage, inner]
 
@@ -352,12 +373,25 @@
         route(stage)
         if stage:
             column_copy(zsend, zrecv, z_sems, stage).wait_recv()
-        spread(stage, zrecv, dsend, drecv, d_sems)
+        spread(stage, picks_of[stage], zrecv, dsend, drecv, d_sems)
+
+    def spread_nearer(first):
+        stage = jnp.where(outer == first, 1, 2)
+        near, far = (picks_of[1], picks_of[2]) if first else (picks_of[2], picks_of[1])
+        picks = jnp.where(outer, near.astype(jnp.float32), far.astype(jnp.float32))
+        remote(
+            zsend.at[0],
+            zrecv.at[stage],
+            z_sems.at[0],
+            z_sems.at[stage],
+            plane_peer(1)[1],
+        ).wait_recv()
+        spread(stage, picks.astype(jnp.bfloat16), zrecv, dsend, drecv, d_sems)
 
     def spread_heads(stage):
         if stage:
             column_copy(hsend, hrecv, h_sems, stage).wait_recv()
-        spread(stage, hrecv, esend, erecv, e_sems)
+        spread(stage, picks_of[stage], hrecv, esend, erecv, e_sems)
 
     for small in smalls[4:]:
         small.wait()
@@ -388,7 +422,9 @@
     queries = rotated(rounded(query_w))
     for head in range(heads):
         query_heads[head] = queries[:, head_lanes(head)]
-    for block in range(blocks):
+    send_tokens(1, True)
+    send_tokens(2, False)
+    for block in range(2, blocks):
         if block == blocks - 2:
             weight_copies[3].start()
         state_in(block).start()
@@ -446,11 +482,13 @@
 
     with jax.named_scope("spread_tokens_0"):
         spread_tokens(0)
-    column_copy(zsend, zrecv, z_sems, 3).start()
     with jax.named_scope("read_a"):
         lax.fori_loop(0, blocks // 2, read, 0)
-    with jax.named_scope("spread_tokens_1"):
-        spread_tokens(1)
+    send_tokens(3, True)
+    with jax.named_scope("spread_near"):
+        for stage in (1, 2):
+            route(stage)
+        spread_nearer(True)
     with jax.named_scope("read"):
         lax.fori_loop(blocks // 2, blocks, read, 0)
     for copy in weight_copies[4:] + loads:
@@ -472,89 +510,96 @@
     hsend[...] = dot(placing, mixed_heads).astype(jnp.bfloat16).reshape(hsend.shape)
     each_column(lambda step: column_copy(hsend, hrecv, h_sems, step).start())
     hrecv[0] = hsend[group]
-    for block in range(blocks):
-        key_columns[block] = keys[block * BLOCK : (block + 1) * BLOCK].T
-    with jax.named_scope("spread_heads_0"):
-        spread_heads(0)
-    advance(0, blocks // 6)
-    with jax.named_scope("spread_tokens_2"):
-        spread_tokens(2)
-    for stage in ORDER[:2]:
-        with jax.named_scope(f"spread_heads_{stage}"):
-            spread_heads(stage)
-    with jax.named_scope("wait_oe"):
-        for copy in weight_copies[4:] + loads:
-            copy.wait()
-
-    def run_expert(stage):
+    half_width = width // HALVES
+
+    def run_expert(stage, send):
         plane_total(dsend, drecv, d_sems, stage).wait_recv()
+        token_rows = unstacked(dot(packing, load_packed(drecv, stage)))
         plane_total(esend, erecv, e_sems, stage).wait_recv()
-        token_rows = unstacked(dot(packing, load_packed(drecv, stage)))
         head_rows = unstacked(dot(packing, load_packed(erecv, stage))).astype(jnp.bfloat16)
         block = (token_rows + dot(head_rows, out_w[...])).astype(jnp.bfloat16)
         block = rms(block.astype(jnp.float32), moe_gain[...]).astype(jnp.bfloat16)
         hidden = jax.nn.silu(dot(block, expert_gate_w[...])) * dot(block, expert_up_w[...])
-        block = dot(hidden.astype(jnp.bfloat16), expert_down_w[...]).astype(jnp.bfloat16)
-        store_packed(osend, stage, take(packing, stacked(block)))
-
-    def send_back(stage):
-        each_plane(lambda step: plane_copy(osend, orecv, o_sems, stage, step).start())
-        orecv[stage, inner] = osend[stage, inner]
-
-    def combine(stage):
-        plane_total(osend, orecv, o_sems, stage).wait_recv()
-        block = load_packed(orecv, stage)
+        hidden = hidden.astype(jnp.bfloat16)
+        for half in range(HALVES):
+            lanes = slice(half * half_width, (half + 1) * half_width)
+            block = dot(hidden, expert_down_w[:, lanes]).astype(jnp.bfloat16)
+            store_packed(osend, stage * HALVES + half, take(packing, stacked(block)))
+            if send:
+                send_back(stage, half)
+
+    def send_back(stage, half):
+        index = stage * HALVES + half
+        each_plane(lambda step: plane_copy(osend, orecv, o_sems, index, step).start())
+        orecv[index, inner] = osend[index, inner]
+
+    def combine(stage, half):
+        index = stage * HALVES + half
+        plane_total(osend, orecv, o_sems, index).wait_recv()
+        block = load_packed(orecv, index)
         high, low = weights_of[stage]
-        csend[stage] = unstacked(dot(high, block) + dot(low, block)).astype(jnp.bfloat16)
+        block = unstacked(dot(high, block) + dot(low, block)).astype(jnp.bfloat16)
         if stage:
-            send_home(stage).start()
+            csend[stage, half] = block
+            send_home(stage, half).start()
         else:
-            crecv[group] = csend[0]
-
-    advance(blocks // 6, 3 * blocks // 6)
+            crecv[group, half] = block
+
+    def combine_all(stage):
+        for half in range(HALVES):
+            with jax.named_scope(f"combine_{stage}_{half}"):
+                combine(stage, half)
+
+    with jax.named_scope("spread_heads_0"):
+        spread_heads(0)
+    with jax.named_scope("spread_far"):
+        spread_nearer(False)
+    send_tokens(3, False)
+    for block in range(blocks):
+        key_columns[block] = keys[block * BLOCK : (block + 1) * BLOCK].T
+    for stage in (2, 1):
+        with jax.named_scope(f"spread_heads_{stage}"):
+            spread_heads(stage)
     with jax.named_scope("spread_tokens_3"):
         spread_tokens(3)
     with jax.named_scope("spread_heads_3"):
         spread_heads(3)
-    with jax.named_scope("run_expert_2"):
-        run_expert(2)
-    send_back(2)
+    with jax.named_scope("wait_oe"):
+        for copy in weight_copies[4:] + loads:
+            copy.wait()
+
+    with jax.named_scope("run_expert_0"):
+        run_expert(0, False)
+    for stage in (2, 3):
+        with jax.named_scope(f"run_expert_{stage}"):
+            run_expert(stage, True)
+    combine_all(2)
     with jax.named_scope("run_expert_1"):
-        run_expert(1)
-    with jax.named_scope("run_expert_3"):
-        run_expert(3)
-    send_back(3)
-    with jax.named_scope("combine_2"):
-        combine(2)
-    send_back(1)
-    with jax.named_scope("run_expert_0"):
-        run_expert(0)
-    send_back(0)
-    with jax.named_scope("combine_3"):
-        combine(3)
-    advance(3 * blocks // 6, 4 * blocks // 6)
-    with jax.named_scope("combine_1"):
-        combine(1)
-    advance(4 * blocks // 6, blocks)
-    with jax.named_scope("combine_0"):
-        combine(0)
+        run_expert(1, True)
+    combine_all(3)
+    for half in range(HALVES):
+        send_back(0, half)
     with jax.named_scope("mixed"):
         mixed = (inputs + dot(mixed_heads, out_w[...])).astype(jnp.bfloat16)
-    with jax.named_scope("wait_home"):
-        each_column(lambda step: send_home(step).wait_recv())
+    advance(0, 2 * blocks // 3)
+    combine_all(1)
+    combine_all(0)
+    advance(2 * blocks // 3, blocks)
     slot_across = lax.broadcasted_iota(jnp.int32, (seq_count, slots), 1).astype(jnp.float32)
     collecting = (slot_across == column(group_slot)).astype(jnp.float32).astype(jnp.bfloat16)
-    block = dot(collecting, crecv[...].reshape(slots, width))
-    out[...] = (mixed.astype(jnp.float32) + block).astype(jnp.bfloat16)
-    each_column(lambda step: column_copy(meta_send, meta_recv, meta_sems, step).wait_send())
-    each_column(lambda step: column_copy(zsend, zrecv, z_sems, step).wait_send())
-    each_column(lambda step: column_copy(hsend, hrecv, h_sems, step).wait_send())
-    each_column(lambda step: send_home(step).wait_send())
-
-    for stage in range(STAGES):
-        plane_total(dsend, drecv, d_sems, stage).wait_send()
-        plane_total(esend, erecv, e_sems, stage).wait_send()
-        plane_total(osend, orecv, o_sems, stage).wait_send()
+    for half in range(HALVES):
+        lanes = slice(half * half_width, (half + 1) * half_width)
+        with jax.named_scope(f"wait_home_{half}"):
+            each_column(lambda step: send_home(step, half).wait_recv())
+        block = dot(collecting, crecv[:, half].reshape(slots, half_width))
+        out[:, lanes] = (mixed[:, lanes].astype(jnp.float32) + block).astype(jnp.bfloat16)
+    column_sent(meta_send, meta_recv, meta_sems).wait_send()
+    column_sent(zsend, zrecv, z_sems).wait_send()
+    column_sent(hsend, hrecv, h_sems).wait_send()
+    column_sent(csend, crecv, c_sems).wait_send()
+    plane_sent(dsend, drecv, d_sems).wait_send()
+    plane_sent(esend, erecv, e_sems).wait_send()
+    plane_sent(osend, orecv, o_sems).wait_send()
 
 
 def finish_kernel(output, state, out, state_out, sem):
@@ -620,6 +665,7 @@
     group_rows = -(-min(seq_count, per_group * capacity // TOP_K) // 8) * 8
     capacity += capacity % 2
     packed = capacity * QUARTERS // BLOCK
+    half_lanes = model_width // HALVES * packed // QUARTERS
     vmem = pl.BlockSpec(memory_space=pltpu.VMEM)
     smem = pl.BlockSpec(memory_space=pltpu.SMEM)
     hbm = pl.BlockSpec(memory_space=pl.ANY)
@@ -673,20 +719,20 @@
         + column_buffer(mixed_width)
         + plane_buffer(model_width)
         + plane_buffer(mixed_width)
-        + plane_buffer(model_width)
-        + column_buffer(model_width)
+        + [pltpu.VMEM((STAGES * HALVES, per_group, BLOCK, half_lanes), bf16)] * 2
+        + [pltpu.VMEM((GROUPS, HALVES, group_rows, model_width // HALVES), bf16)] * 2
         + [
             dma((9,)),
             dma((5,)),
             dma((blocks,)),
             dma((3,)),
-            dma((2, GROUPS)),
-            dma((2, GROUPS)),
-            dma((2, GROUPS)),
-            dma((2, STAGES)),
-            dma((2, STAGES)),
-            dma((2, STAGES)),
-            dma((2, STAGES)),
+            dma((GROUPS,)),
+            dma((GROUPS,)),
+            dma((GROUPS,)),
+            dma((STAGES + 1,)),
+            dma((STAGES + 1,)),
+            dma((STAGES * HALVES + 1,)),
+            dma((GROUPS * HALVES,)),
         ],
         compiler_params=pltpu.CompilerParams(
             collective_id=0,

time: 45.8 us -> 44.9 us (0.980)
  Pallas kernels: 45 us -> 44.1 us
    pallas_call x1, Pallas kernels: 40.2 us -> 39.4 us  [local(): pl.pallas_call(kernel, name='layer', out_shape=(pltpu.VMEM((seq_count, mo...]
where the time goes in v4:
time: 44.9 us; the launch traced here: 44.7 us
  Pallas kernels  44.1 us (98%)
  between operations  0.65 us (1%)
    pallas_call x1, Pallas kernels, local(): pl.pallas_call(kernel, name='layer', out_shape=(pltpu.VMEM((seq_count, mo...  39.4 us
    pallas_call x1, Pallas kernels, finish(): pl.pallas_call(finish_kernel, name='finish', out_shape=(jax.ShapeDtypeStr...  4.74 us

profile of v4, /device:TPU:0, one launch (start us, length us, event | category | flops | bytes accessed | tf_op | source)
XLA Modules:
  0.0 44.7 jit_solution(17926575001023014551)
XLA Ops:
  0.6 39.4 %layer.1 = (bf16[48,2048]{1,0:T(8,128)(2,1)S(1)}, f32[48,8,64,64]{3,2,1,0:T(8,128)S(1)}) custom-call(f32[8]{0:T(128)} %refs_0_.1, bf16[48,2048]{1,0:T(8,128)(2,1)} %refs_1_.1, s32[1,48]{1,0:T(1,128)} %bitcast.18, f32[1,32]{1,0:T(1,128)} %constant.2.clone.refs_3_, f32[1,2048]{1,0:T(1,128)} %bitcast.13, f32[1,512]{1,0:T(1,128)} %bitcast.15, ...), custom_call_target="tpu_custom_call" | custom-call | tf_op jit(solution)/shard_map/layer/pallas_call | solution.py:699
  40.0 4.7 %finish.1 = (bf16[48,2048]{1,0:T(8,128)(2,1)}, f32[48,8,64,64]{3,2,1,0:T(8,128)}) custom-call(bf16[48,2048]{1,0:T(8,128)(2,1)S(1)} %get-tuple-element.4.output, f32[48,8,64,64]{3,2,1,0:T(8,128)S(1)} %get-tuple-element.5.state), custom_call_target="tpu_custom_call" | custom-call | tf_op jit(solution)/shard_map/finish/pallas_call | solution.py:621

commit v5 on v4

--- a/solution.py
+++ b/solution.py
@@ -117,9 +117,13 @@
     half = head_width // 2
     blocks = seq_count // BLOCK
 
+    side = group // 2
+    within = group * (GROUPS - 1 - group) // 2
+    others = {1: group + 1 - 2 * (group % 2), 2: 3 * (1 - side), 3: 2 - side}
+    landing = {1: 1, 2: 2 + within, 3: 2 + within}
+
     def column_peer(step):
-        other = {1: group + 1 - 2 * (group % 2), 2: (group + 2) % GROUPS, 3: GROUPS - 1 - group}[step]
-        return other, other * per_group + inner
+        return others[step], others[step] * per_group + inner
 
     def plane_peer(step):
         other = lax.rem(inner + step, per_group)
@@ -137,19 +141,31 @@
 
     def column_copy(source, target, sems, step):
         other, peer = column_peer(step)
-        return remote(source.at[other], target.at[step], sems.at[0], sems.at[step], peer)
+        place = landing[step]
+        return remote(source.at[other], target.at[place], sems.at[0], sems.at[place], peer)
+
+    def column_landed(source, target, sems, step):
+        return remote(source.at[0], target.at[step], sems.at[0], sems.at[step], column_peer(1)[1])
 
     def column_sent(source, target, sems):
         others = pl.ds(1, GROUPS - 1)
         return remote(source.at[others], target.at[others], sems.at[0], sems.at[1], column_peer(1)[1])
 
     def send_home(step, half):
-        index = step * HALVES + half
         return remote(
             csend.at[step, half],
             crecv.at[group, half],
             c_sems.at[0],
-            c_sems.at[index],
+            c_sems.at[landing[step] * HALVES + half],
+            column_peer(step)[1],
+        )
+
+    def home_landed(step, half):
+        return remote(
+            csend.at[step, half],
+            crecv.at[step, half],
+            c_sems.at[0],
+            c_sems.at[step * HALVES + half],
             column_peer(step)[1],
         )
 
@@ -268,14 +284,14 @@
     zsend[...] = dot(placing, tokens[...]).astype(jnp.bfloat16).reshape(zsend.shape)
     with jax.named_scope("barrier"):
         pl.semaphore_wait(barrier, GROUPS - 1 + per_group - 1)
-    outer = group * (GROUPS - 1 - group) == 0
+    outer = within == 0
 
     def send_tokens(stage, held):
         @pl.when(outer if held else jnp.logical_not(outer))
         def start():
             column_copy(zsend, zrecv, z_sems, stage).start()
 
-    send_tokens(2, True)
+    send_tokens(3, True)
     send_tokens(1, False)
     for block in range(2):
         state_in(block).start()
@@ -351,7 +367,7 @@
 
     def route(stage):
         if stage:
-            column_copy(meta_send, meta_recv, meta_sems, stage).wait_recv()
+            column_landed(meta_send, meta_recv, meta_sems, stage).wait_recv()
         meta = meta_recv[stage].astype(jnp.float32)
         first = (row_names == meta[:, 0:1]).astype(jnp.float32)
         second = (row_names == meta[:, 1:2]).astype(jnp.float32)
@@ -372,25 +388,19 @@
     def spread_tokens(stage):
         route(stage)
         if stage:
-            column_copy(zsend, zrecv, z_sems, stage).wait_recv()
+            column_landed(zsend, zrecv, z_sems, stage).wait_recv()
         spread(stage, picks_of[stage], zrecv, dsend, drecv, d_sems)
 
     def spread_nearer(first):
         stage = jnp.where(outer == first, 1, 2)
         near, far = (picks_of[1], picks_of[2]) if first else (picks_of[2], picks_of[1])
         picks = jnp.where(outer, near.astype(jnp.float32), far.astype(jnp.float32))
-        remote(
-            zsend.at[0],
-            zrecv.at[stage],
-            z_sems.at[0],
-            z_sems.at[stage],
-            plane_peer(1)[1],
-        ).wait_recv()
+        column_landed(zsend, zrecv, z_sems, stage).wait_recv()
         spread(stage, picks.astype(jnp.bfloat16), zrecv, dsend, drecv, d_sems)
 
     def spread_heads(stage):
         if stage:
-            column_copy(hsend, hrecv, h_sems, stage).wait_recv()
+            column_landed(hsend, hrecv, h_sems, stage).wait_recv()
         spread(stage, picks_of[stage], hrecv, esend, erecv, e_sems)
 
     for small in smalls[4:]:
@@ -422,7 +432,7 @@
     queries = rotated(rounded(query_w))
     for head in range(heads):
         query_heads[head] = queries[:, head_lanes(head)]
-    send_tokens(1, True)
+    send_tokens(2, True)
     send_tokens(2, False)
     for block in range(2, blocks):
         if block == blocks - 2:
@@ -482,9 +492,10 @@
 
     with jax.named_scope("spread_tokens_0"):
         spread_tokens(0)
+    send_tokens(3, False)
     with jax.named_scope("read_a"):
         lax.fori_loop(0, blocks // 2, read, 0)
-    send_tokens(3, True)
+    send_tokens(1, True)
     with jax.named_scope("spread_near"):
         for stage in (1, 2):
             route(stage)
@@ -512,7 +523,7 @@
     hrecv[0] = hsend[group]
     half_width = width // HALVES
 
-    def run_expert(stage, send):
+    def run_expert(stage):
         plane_total(dsend, drecv, d_sems, stage).wait_recv()
         token_rows = unstacked(dot(packing, load_packed(drecv, stage)))
         plane_total(esend, erecv, e_sems, stage).wait_recv()
@@ -525,7 +536,10 @@
             lanes = slice(half * half_width, (half + 1) * half_width)
             block = dot(hidden, expert_down_w[:, lanes]).astype(jnp.bfloat16)
             store_packed(osend, stage * HALVES + half, take(packing, stacked(block)))
-            if send:
+            if stage > 1:
+                send_back(stage, half)
+        if stage == 1:
+            for half in range(HALVES):
                 send_back(stage, half)
 
     def send_back(stage, half):
@@ -554,43 +568,42 @@
         spread_heads(0)
     with jax.named_scope("spread_far"):
         spread_nearer(False)
-    send_tokens(3, False)
     for block in range(blocks):
         key_columns[block] = keys[block * BLOCK : (block + 1) * BLOCK].T
+    advance(0, blocks // 3)
     for stage in (2, 1):
         with jax.named_scope(f"spread_heads_{stage}"):
             spread_heads(stage)
     with jax.named_scope("spread_tokens_3"):
         spread_tokens(3)
-    with jax.named_scope("spread_heads_3"):
-        spread_heads(3)
     with jax.named_scope("wait_oe"):
         for copy in weight_copies[4:] + loads:
             copy.wait()
 
     with jax.named_scope("run_expert_0"):
-        run_expert(0, False)
-    for stage in (2, 3):
+        run_expert(0)
+    with jax.named_scope("spread_heads_3"):
+        spread_heads(3)
+    for stage in (2, 1, 3):
         with jax.named_scope(f"run_expert_{stage}"):
-            run_expert(stage, True)
+            run_expert(stage)
     combine_all(2)
-    with jax.named_scope("run_expert_1"):
-        run_expert(1, True)
-    combine_all(3)
     for half in range(HALVES):
         send_back(0, half)
+    combine_all(1)
     with jax.named_scope("mixed"):
         mixed = (inputs + dot(mixed_heads, out_w[...])).astype(jnp.bfloat16)
-    advance(0, 2 * blocks // 3)
-    combine_all(1)
+    advance(blocks // 3, blocks // 2)
+    combine_all(3)
+    advance(blocks // 2, 5 * blocks // 6)
     combine_all(0)
-    advance(2 * blocks // 3, blocks)
+    advance(5 * blocks // 6, blocks)
     slot_across = lax.broadcasted_iota(jnp.int32, (seq_count, slots), 1).astype(jnp.float32)
     collecting = (slot_across == column(group_slot)).astype(jnp.float32).astype(jnp.bfloat16)
     for half in range(HALVES):
         lanes = slice(half * half_width, (half + 1) * half_width)
         with jax.named_scope(f"wait_home_{half}"):
-            each_column(lambda step: send_home(step, half).wait_recv())
+            each_column(lambda step: home_landed(step, half).wait_recv())
         block = dot(collecting, crecv[:, half].reshape(slots, half_width))
         out[:, lanes] = (mixed[:, lanes].astype(jnp.float32) + block).astype(jnp.bfloat16)
     column_sent(meta_send, meta_recv, meta_sems).wait_send()

time: 44.9 us -> 42.1 us (0.938)
  Pallas kernels: 44.1 us -> 41.3 us
    pallas_call x1, Pallas kernels: 39.4 us -> 36.6 us  [local(): pl.pallas_call(kernel, name='layer', out_shape=(pltpu.VMEM((seq_count, mo...]
where the time goes in v5:
time: 42.1 us; the launch traced here: 41.9 us
  Pallas kernels  41.3 us (98%)
  between operations  0.65 us (2%)
    pallas_call x1, Pallas kernels, local(): pl.pallas_call(kernel, name='layer', out_shape=(pltpu.VMEM((seq_count, mo...  36.6 us
    pallas_call x1, Pallas kernels, finish(): pl.pallas_call(finish_kernel, name='finish', out_shape=(jax.ShapeDtypeStr...  4.74 us

profile of v5, /device:TPU:0, one launch (start us, length us, event | category | flops | bytes accessed | tf_op | source)
XLA Modules:
  0.0 41.9 jit_solution(14543635973397888419)
XLA Ops:
  0.6 36.6 %layer.1 = (bf16[48,2048]{1,0:T(8,128)(2,1)S(1)}, f32[48,8,64,64]{3,2,1,0:T(8,128)S(1)}) custom-call(f32[8]{0:T(128)} %refs_0_.1, bf16[48,2048]{1,0:T(8,128)(2,1)} %refs_1_.1, s32[1,48]{1,0:T(1,128)} %bitcast.18, f32[1,32]{1,0:T(1,128)} %constant.2.clone.refs_3_, f32[1,2048]{1,0:T(1,128)} %bitcast.13, f32[1,512]{1,0:T(1,128)} %bitcast.15, ...), custom_call_target="tpu_custom_call" | custom-call | tf_op jit(solution)/shard_map/layer/pallas_call | solution.py:712
  37.2 4.7 %finish.1 = (bf16[48,2048]{1,0:T(8,128)(2,1)}, f32[48,8,64,64]{3,2,1,0:T(8,128)}) custom-call(bf16[48,2048]{1,0:T(8,128)(2,1)S(1)} %get-tuple-element.4.output, f32[48,8,64,64]{3,2,1,0:T(8,128)S(1)} %get-tuple-element.5.state), custom_call_target="tpu_custom_call" | custom-call | tf_op jit(solution)/shard_map/finish/pallas_call | solution.py:634

commit v6 on v5

--- a/solution.py
+++ b/solution.py
@@ -523,24 +523,29 @@
     hrecv[0] = hsend[group]
     half_width = width // HALVES
 
-    def run_expert(stage):
-        plane_total(dsend, drecv, d_sems, stage).wait_recv()
-        token_rows = unstacked(dot(packing, load_packed(drecv, stage)))
-        plane_total(esend, erecv, e_sems, stage).wait_recv()
-        head_rows = unstacked(dot(packing, load_packed(erecv, stage))).astype(jnp.bfloat16)
+    def run_expert(*stages):
+        token_rows, head_rows = [], []
+        for stage in stages:
+            plane_total(dsend, drecv, d_sems, stage).wait_recv()
+            token_rows.append(unstacked(dot(packing, load_packed(drecv, stage))))
+        for stage in stages:
+            plane_total(esend, erecv, e_sems, stage).wait_recv()
+            head_rows.append(unstacked(dot(packing, load_packed(erecv, stage))))
+        head_rows = jnp.concatenate(head_rows, axis=0).astype(jnp.bfloat16)
+        token_rows = jnp.concatenate(token_rows, axis=0)
         block = (token_rows + dot(head_rows, out_w[...])).astype(jnp.bfloat16)
         block = rms(block.astype(jnp.float32), moe_gain[...]).astype(jnp.bfloat16)
         hidden = jax.nn.silu(dot(block, expert_gate_w[...])) * dot(block, expert_up_w[...])
         hidden = hidden.astype(jnp.bfloat16)
         for half in range(HALVES):
             lanes = slice(half * half_width, (half + 1) * half_width)
-            block = dot(hidden, expert_down_w[:, lanes]).astype(jnp.bfloat16)
-            store_packed(osend, stage * HALVES + half, take(packing, stacked(block)))
-            if stage > 1:
-                send_back(stage, half)
-        if stage == 1:
-            for half in range(HALVES):
-                send_back(stage, half)
+            block = dot(hidden, expert_down_w[:, lanes])
+            for place, stage in enumerate(stages):
+                share = block[place * rows : (place + 1) * rows].astype(jnp.bfloat16)
+                store_packed(osend, stage * HALVES + half, take(packing, stacked(share)))
+            if stages[0]:
+                for stage in stages:
+                    send_back(stage, half)
 
     def send_back(stage, half):
         index = stage * HALVES + half
@@ -584,18 +589,21 @@
         run_expert(0)
     with jax.named_scope("spread_heads_3"):
         spread_heads(3)
-    for stage in (2, 1, 3):
-        with jax.named_scope(f"run_expert_{stage}"):
-            run_expert(stage)
+    with jax.named_scope("run_expert_2"):
+        run_expert(2)
+    with jax.named_scope("run_expert_31"):
+        run_expert(1, 3)
     combine_all(2)
     for half in range(HALVES):
         send_back(0, half)
-    combine_all(1)
     with jax.named_scope("mixed"):
         mixed = (inputs + dot(mixed_heads, out_w[...])).astype(jnp.bfloat16)
     advance(blocks // 3, blocks // 2)
-    combine_all(3)
-    advance(blocks // 2, 5 * blocks // 6)
+    for half in range(HALVES):
+        for stage in (1, 3):
+            with jax.named_scope(f"combine_{stage}_{half}"):
+                combine(stage, half)
+        advance((3 + half) * blocks // 6, (4 + half) * blocks // 6)
     combine_all(0)
     advance(5 * blocks // 6, blocks)
     slot_across = lax.broadcasted_iota(jnp.int32, (seq_count, slots), 1).astype(jnp.float32)

time: 42.1 us -> 41.5 us (0.986)
  Pallas kernels: 41.3 us -> 40.7 us
    pallas_call x1, Pallas kernels: 36.6 us -> 36 us  [local(): pl.pallas_call(kernel, name='layer', out_shape=(pltpu.VMEM((seq_count, mo...]
where the time goes in v6:
time: 41.5 us; the launch traced here: 41.4 us
  Pallas kernels  40.7 us (98%)
  between operations  0.65 us (2%)
    pallas_call x1, Pallas kernels, local(): pl.pallas_call(kernel, name='layer', out_shape=(pltpu.VMEM((seq_count, mo...  36 us
    pallas_call x1, Pallas kernels, finish(): pl.pallas_call(finish_kernel, name='finish', out_shape=(jax.ShapeDtypeStr...  4.74 us

profile of v6, /device:TPU:0, one launch (start us, length us, event | category | flops | bytes accessed | tf_op | source)
XLA Modules:
  0.0 41.4 jit_solution(14253378578135807813)
XLA Ops:
  0.6 36.0 %layer.1 = (bf16[48,2048]{1,0:T(8,128)(2,1)S(1)}, f32[48,8,64,64]{3,2,1,0:T(8,128)S(1)}) custom-call(f32[8]{0:T(128)} %refs_0_.1, bf16[48,2048]{1,0:T(8,128)(2,1)} %refs_1_.1, s32[1,48]{1,0:T(1,128)} %bitcast.18, f32[1,32]{1,0:T(1,128)} %constant.2.clone.refs_3_, f32[1,2048]{1,0:T(1,128)} %bitcast.13, f32[1,512]{1,0:T(1,128)} %bitcast.15, ...), custom_call_target="tpu_custom_call" | custom-call | tf_op jit(solution)/shard_map/layer/pallas_call | solution.py:720
  36.6 4.7 %finish.1 = (bf16[48,2048]{1,0:T(8,128)(2,1)}, f32[48,8,64,64]{3,2,1,0:T(8,128)}) custom-call(bf16[48,2048]{1,0:T(8,128)(2,1)S(1)} %get-tuple-element.4.output, f32[48,8,64,64]{3,2,1,0:T(8,128)S(1)} %get-tuple-element.5.state), custom_call_target="tpu_custom_call" | custom-call | tf_op jit(solution)/shard_map/finish/pallas_call | solution.py:642

commit v7 on v6

--- a/solution.py
+++ b/solution.py
@@ -575,7 +575,7 @@
         spread_nearer(False)
     for block in range(blocks):
         key_columns[block] = keys[block * BLOCK : (block + 1) * BLOCK].T
-    advance(0, blocks // 3)
+    advance(0, blocks // 2)
     for stage in (2, 1):
         with jax.named_scope(f"spread_heads_{stage}"):
             spread_heads(stage)
@@ -598,14 +598,13 @@
         send_back(0, half)
     with jax.named_scope("mixed"):
         mixed = (inputs + dot(mixed_heads, out_w[...])).astype(jnp.bfloat16)
-    advance(blocks // 3, blocks // 2)
+    advance(blocks // 2, 4 * blocks // 6)
     for half in range(HALVES):
         for stage in (1, 3):
             with jax.named_scope(f"combine_{stage}_{half}"):
                 combine(stage, half)
-        advance((3 + half) * blocks // 6, (4 + half) * blocks // 6)
+        advance((4 + half) * blocks // 6, (5 + half) * blocks // 6)
     combine_all(0)
-    advance(5 * blocks // 6, blocks)
     slot_across = lax.broadcasted_iota(jnp.int32, (seq_count, slots), 1).astype(jnp.float32)
     collecting = (slot_across == column(group_slot)).astype(jnp.float32).astype(jnp.bfloat16)
     for half in range(HALVES):

time: 41.5 us -> 41.9 us (level)
  no operation moved by 1% of the time
where the time goes in v7:
time: 41.9 us; the launch traced here: 41.8 us
  Pallas kernels  41.1 us (98%)
  between operations  0.65 us (2%)
    pallas_call x1, Pallas kernels, local(): pl.pallas_call(kernel, name='layer', out_shape=(pltpu.VMEM((seq_count, mo...  36.4 us
    pallas_call x1, Pallas kernels, finish(): pl.pallas_call(finish_kernel, name='finish', out_shape=(jax.ShapeDtypeStr...  4.74 us

profile of v7, /device:TPU:0, one launch (start us, length us, event | category | flops | bytes accessed | tf_op | source)
XLA Modules:
  0.0 41.8 jit_solution(4697993141884337966)
XLA Ops:
  0.6 36.4 %layer.1 = (bf16[48,2048]{1,0:T(8,128)(2,1)S(1)}, f32[48,8,64,64]{3,2,1,0:T(8,128)S(1)}) custom-call(f32[8]{0:T(128)} %refs_0_.1, bf16[48,2048]{1,0:T(8,128)(2,1)} %refs_1_.1, s32[1,48]{1,0:T(1,128)} %bitcast.18, f32[1,32]{1,0:T(1,128)} %constant.2.clone.refs_3_, f32[1,2048]{1,0:T(1,128)} %bitcast.13, f32[1,512]{1,0:T(1,128)} %bitcast.15, ...), custom_call_target="tpu_custom_call" | custom-call | tf_op jit(solution)/shard_map/layer/pallas_call | solution.py:719
  37.0 4.7 %finish.1 = (bf16[48,2048]{1,0:T(8,128)(2,1)}, f32[48,8,64,64]{3,2,1,0:T(8,128)}) custom-call(bf16[48,2048]{1,0:T(8,128)(2,1)S(1)} %get-tuple-element.4.output, f32[48,8,64,64]{3,2,1,0:T(8,128)S(1)} %get-tuple-element.5.state), custom_call_target="tpu_custom_call" | custom-call | tf_op jit(solution)/shard_map/finish/pallas_call | solution.py:641
